TPU v7x, 32 devices: a whole 2x2x4 slice. The times are simulated.
32 devices in a mesh: fs: 8 (over z, y), tp: 4 (over x, core).
Axes of the slice: x: 2, y: 2, z: 4, core: 2. Of those that a mesh axis runs over, the one named last changes fastest.
Arguments:
- stream_in: bfloat16 [2048, 2112], P('fs'), may hold values from -6 to 6
- norm_gains: float32 [6, 2112], replicated, may hold values from 0.1 to 1.9
- gate_proj: bfloat16 [2112, 3072], P('fs', 'tp'), may hold values from -0.125 to 0.125
- up_proj: bfloat16 [2112, 3072], P('fs', 'tp'), may hold values from -0.125 to 0.125
- down_proj: bfloat16 [2112, 3072], P('fs', 'tp'), may hold values from -0.109375 to 0.109375
- outer_gate: bfloat16 [2112, 1056], P('fs', 'tp'), may hold values from -0.125 to 0.125
- inner_gate: bfloat16 [2112, 1056], P('fs', 'tp'), may hold values from -0.125 to 0.125
- value_proj: bfloat16 [2112, 1056], P('fs', 'tp'), may hold values from -0.125 to 0.125
- mixer_out: bfloat16 [2112, 1056], P('fs', 'tp'), may hold values from -0.1875 to 0.1875
- conv_taps: bfloat16 [3, 1056], replicated, may hold values from -3 to 3
Outputs:
- stream_out: bfloat16 [2048, 2112], P('fs')
All inputs are finite; a program needn't handle non-finite values.
Results may differ from a plain program's by a relative error of at most 0.02.
Values may be sent and summed in bfloat16 or wider, within the bound.
A program may use at most 64 MiB of HBM per device.

v0:
```python
import functools

import jax
import jax.numpy as jnp
from jax import lax
from jax.experimental import pallas as pl
from jax.experimental.pallas import tpu as pltpu
from jax.sharding import PartitionSpec as P

MESH = pl.DeviceIdType.MESH
EPSILON = 1e-06
CONV_K = 3
F32, BF16 = jnp.float32, jnp.bfloat16
NT = (((1,), (1,)), ((), ()))


def kernel(cfg, *refs):
    Z, Y, X, shard, sent, width, hc, nff, main, rem = cfg
    own_refs = refs[:8]
    stream_ref, gains_ref, taps_ref, out_ref = refs[8:12]
    (ff, g3, g4, normed, acc, hidden, csend, crecv, xsend, xrecv, res,
     lsem, zsend, recv, asend, arecv, csem, xssem, xrsem, rsem) = refs[12:]
    rows, Dp = stream_ref.shape
    half, quarter = rows // 2, rows // 4
    K3, K4 = nff, nff + 1
    f, t = lax.axis_index("fs"), lax.axis_index("tp")
    z, y = f // Y, f % Y
    c, x = t % 2, t // 2
    core_peer = (f, x * 2 + 1 - c)
    x_peers = [(f, ((x + j) % X) * 2 + c) for j in range(1, X)]

    def dev_z(zz):
        return (zz * Y + y, t)

    dev_y = (z * Y + (Y - 1 - y), t)

    for s in range(Z * Y):
        tail = pl.ds(s * shard + shard - 16, 16)
        for k in range(nff):
            ff[k, tail] = jnp.zeros((16, 3 * hc), BF16)
        g3[tail] = jnp.zeros((16, 2 * main), BF16)
        g4[tail] = jnp.zeros((16, 2 * main + 128), BF16)

    barrier = pltpu.get_barrier_semaphore()

    def greet(d):
        pl.semaphore_signal(barrier, inc=1, device_id=d, device_id_type=MESH)

    always = [core_peer] + x_peers + ([dev_y] if Y == 2 else [])
    for d in always:
        greet(d)
    if Z > 1:
        @pl.when(z > 0)
        def _():
            greet(dev_z(z - 1))

        @pl.when(z < Z - 1)
        def _():
            greet(dev_z(z + 1))

    def slot(k, first, count):
        at = pl.ds(pl.multiple_of(first * shard, 16), (count - 1) * shard + sent)
        if k < nff:
            return ff.at[k, at]
        return (g3 if k == K3 else g4).at[at]

    here = pl.ds(pl.multiple_of(f * shard, 16), sent)
    moves = []
    for k in range(nff):
        for j in range(3):
            moves.append((k, own_refs[j].at[:, pl.ds(k * hc, hc)],
                          ff.at[k, here, pl.ds(j * hc, hc)]))
    ow, iw, vw, mw, rw = own_refs[3:]
    lead = pl.ds(0, main)
    moves.append((K3, ow.at[:, lead], g3.at[here, lead]))
    moves.append((K3, iw.at[:, lead], g3.at[here, pl.ds(main, main)]))
    moves.append((K4, vw.at[:, lead], g4.at[here, lead]))
    moves.append((K4, rw, g4.at[here, pl.ds(main, 128)]))
    moves.append((K4, mw.at[:, lead], g4.at[here, pl.ds(main + 128, main)]))
    local = [
        (k, pltpu.make_async_copy(src, dst, lsem.at[n])) for n, (k, src, dst) in enumerate(moves)
    ]
    for _, copy in local:
        copy.start()

    peers = len(always)
    if Z > 1:
        peers = peers + (z > 0).astype(jnp.int32) + (z < Z - 1).astype(jnp.int32)
    pl.semaphore_wait(barrier, peers)

    def remote(k, s, way, d):
        ref = slot(k, s, 1)
        return pltpu.make_async_remote_copy(
            src_ref=ref, dst_ref=ref, send_sem=zsend.at[k, way, s], recv_sem=recv.at[k, s],
            device_id=d, device_id_type=MESH,
        )

    def remote_a(s, way, d):
        ref = slot(K4, s * Y, Y)
        return pltpu.make_async_remote_copy(
            src_ref=ref, dst_ref=ref, send_sem=asend.at[way, s], recv_sem=arecv.at[s],
            device_id=d, device_id_type=MESH,
        )

    def right(k, s, act):
        @pl.when(z < Z - 1)
        def _():
            act(remote(k, s * Y + y, 0, dev_z(z + 1)))

    def left(k, s, act):
        @pl.when(z > 0)
        def _():
            act(remote(k, s * Y + y, 1, dev_z(z - 1)))

    def across(k, s, act):
        if Y == 2:
            act(remote(k, s * Y + y, 2, dev_y))

    def go(copy):
        copy.start()

    def own(k):
        right(k, z, go)
        left(k, z, go)
        across(k, z, go)

    def zsteps(k):
        def step(i, carry):
            @pl.when(z - 1 - i >= 0)
            def _():
                s = z - 1 - i
                remote(k, s * Y + y, 0, dev_z(z - 1)).wait_recv()
                right(k, s, go)
                across(k, s, go)

            @pl.when(z + 1 + i < Z)
            def _():
                s = z + 1 + i
                remote(k, s * Y + y, 0, dev_z(z + 1)).wait_recv()
                left(k, s, go)
                across(k, s, go)

            return carry

        lax.fori_loop(0, Z - 1, step, 0)

    def wait_across(k):
        if Y == 2:
            def step(s, carry):
                remote(k, s * Y + 1 - y, 2, dev_y).wait_recv()
                return carry

            lax.fori_loop(0, Z, step, 0)

    def right_a(s, act):
        @pl.when(z < Z - 1)
        def _():
            act(remote_a(s, 0, dev_z(z + 1)))

    def left_a(s, act):
        @pl.when(z > 0)
        def _():
            act(remote_a(s, 1, dev_z(z - 1)))

    def start_a():
        if Y == 2:
            remote(K4, z * Y + 1 - y, 2, dev_y).wait_recv()
        right_a(z, go)
        left_a(z, go)

    def steps_a(forward):
        def step(i, carry):
            @pl.when((z - 1 - i >= 0) & ((z < Z - 1) if forward else (z == Z - 1)))
            def _():
                s = z - 1 - i
                remote_a(s, 0, dev_z(z - 1)).wait_recv()
                if forward:
                    right_a(s, go)

            @pl.when((z + 1 + i < Z) & ((z > 0) if forward else (z == 0)))
            def _():
                s = z + 1 + i
                remote_a(s, 0, dev_z(z + 1)).wait_recv()
                if forward:
                    left_a(s, go)

            return carry

        lax.fori_loop(0, Z - 1, step, 0)

    def scaled(values, row):
        mean = jnp.sum(values * values, axis=-1, keepdims=True) * (1.0 / width)
        return values * lax.rsqrt(mean + EPSILON) * gains_ref[row : row + 1, :]

    def norm_to(source, row):
        def block(i, carry):
            at = pl.ds(pl.multiple_of(i * 32, 32), 32)
            per_half, per_quarter = half // 32, quarter // 32
            h, b = i // per_half, (i % per_half) // per_quarter
            to = pl.ds(pl.multiple_of(h * quarter + (i % per_quarter) * 32, 32), 32)
            normed[b, to] = scaled(source[at].astype(F32), row).astype(BF16)
            return carry

        lax.fori_loop(0, rows // 32, block, 0)

    def ffn_block(k, b, first):
        weights = ff.at[k]
        n = normed[b]
        gate = jnp.dot(n, weights[:, 0:hc], preferred_element_type=F32)
        up = jnp.dot(n, weights[:, hc : 2 * hc], preferred_element_type=F32)
        h = (gate / (1.0 + jnp.exp(-gate)) * up).astype(BF16)
        part = lax.dot_general(h, weights[:, 2 * hc :], NT, preferred_element_type=F32)
        acc[b] = part if first else acc[b] + part

    def ffn_chunk(k, first):
        def block(b, carry):
            ffn_block(k, b, first)
            return carry

        lax.fori_loop(0, 2, block, 0)

    mine = pl.ds(pl.multiple_of(c * quarter, 16), quarter)
    other = pl.ds(pl.multiple_of((1 - c) * quarter, 16), quarter)

    def core_copy(r, b):
        return pltpu.make_async_remote_copy(
            src_ref=csend.at[r, b], dst_ref=crecv.at[r, b], send_sem=csem.at[0, r, b],
            recv_sem=csem.at[1, r, b], device_id=core_peer, device_id_type=MESH,
        )

    def x_copy(r, b, j):
        return pltpu.make_async_remote_copy(
            src_ref=xsend.at[r, b], dst_ref=xrecv.at[r, b, j], send_sem=xssem.at[r, b, j],
            recv_sem=xrsem.at[r, b, j], device_id=x_peers[j], device_id_type=MESH,
        )

    def res_copy(r, b, core):
        at = pl.ds(pl.multiple_of(core * half + b * quarter, 16), quarter)
        return pltpu.make_async_remote_copy(
            src_ref=res.at[r, at], dst_ref=res.at[r, at], send_sem=rsem.at[0, r, b],
            recv_sem=rsem.at[1, r, b], device_id=core_peer, device_id_type=MESH,
        )

    def reduce(r, compute, source, row, factor):
        def send(b, carry):
            compute(b)
            csend[r, b] = acc[b, other].astype(BF16)
            core_copy(r, b).start()
            core_copy(r, b).wait()
            xsend[r, b] = (
                acc[b, mine].astype(BF16).astype(F32) + crecv[r, b].astype(F32)
            ).astype(BF16)
            for j in range(X - 1):
                x_copy(r, b, j).start()
            return carry

        def receive(b, carry):
            for j in range(X - 1):
                x_copy(r, b, j).wait()

            def block(i, inner_carry):
                at = pl.ds(pl.multiple_of(i * 32, 16), 32)
                full = pl.ds(pl.multiple_of(c * half + b * quarter + i * 32, 16), 32)
                total = xsend[r, b, at].astype(F32)
                for j in range(X - 1):
                    total = total + xrecv[r, b, j, at].astype(F32)
                res[r, full] = (
                    source[full].astype(F32) + factor * scaled(total, row)
                ).astype(BF16)
                return inner_carry

            lax.fori_loop(0, quarter // 32, block, 0)
            res_copy(r, b, c).start()
            return carry

        def finish(b, carry):
            res_copy(r, b, c).wait_send()
            res_copy(r, b, 1 - c).wait_recv()
            return carry

        lax.fori_loop(0, 2, send, 0)
        lax.fori_loop(0, 2, receive, 0)
        lax.fori_loop(0, 2, finish, 0)

    def swapped(v):
        q = [v[j * quarter : (j + 1) * quarter] for j in range(4)]
        return jnp.concatenate([q[0], q[2], q[1], q[3]], axis=0)

    def mixer():
        edge = main + 128
        n = swapped(normed[...].reshape(rows, Dp))
        outer_inner = jnp.dot(n, g3[...], preferred_element_type=F32)
        outer_inner = outer_inner.astype(BF16).astype(F32)
        value_rest = jnp.dot(n, g4[:, 0:edge], preferred_element_type=F32)
        value_rest = value_rest.astype(BF16).astype(F32)
        rest = value_rest[:, main:]
        if rem:
            lane = lax.broadcasted_iota(jnp.int32, rest.shape, 1)
            keep = (lane >= 3 * rem) & (lane < 4 * rem)
            rests = [
                jnp.where(keep, pltpu.roll(rest, (3 - j) * rem, 1), 0.0) for j in range(3)
            ]
        else:
            rests = [jnp.zeros_like(rest)] * 3
        outer = jnp.concatenate([rests[0], outer_inner[:, 0:main]], axis=1)
        inner = jnp.concatenate([rests[1], outer_inner[:, main:]], axis=1)
        value = jnp.concatenate([rests[2], value_rest[:, 0:main]], axis=1)
        gated = inner * value
        token = lax.broadcasted_iota(jnp.int32, gated.shape, 0)
        conv = jnp.zeros_like(gated)
        for j in range(CONV_K):
            back = CONV_K - 1 - j
            moved = gated
            if back:
                moved = jnp.where(token >= back, pltpu.roll(gated, back, 0), 0.0)
            conv = conv + taps_ref[j : j + 1, :] * moved
        hidden[...] = swapped((outer * conv).astype(BF16)).reshape(hidden.shape)

    def mixer_block(b):
        acc[b] = lax.dot_general(hidden[b], g4[:, main:], NT, preferred_element_type=F32)

    def last_chunk(b):
        ffn_block(nff - 1, b, nff == 1)

    def second(b):
        acc[b] = jnp.zeros(acc.shape[1:], F32)

        def again(k, carry):
            ffn_block(k, b, False)
            return carry

        lax.fori_loop(0, nff, again, 0)

    for k in range(nff + 2):
        for owner, copy in local:
            if owner == k:
                copy.wait()
        if k < 2:
            own(k)
    norm_to(stream_ref, 0)
    for k in range(nff):
        zsteps(k)
        if k + 2 <= K3:
            own(k + 2)
        if k + 2 == K3:
            across(K4, z, go)
        if k > 0:
            wait_across(k - 1)
            ffn_chunk(k - 1, k == 1)
    zsteps(K3)
    start_a()
    steps_a(True)
    wait_across(nff - 1)
    reduce(0, last_chunk, stream_ref, 1, 0.5)
    norm_to(res.at[0], 2)
    wait_across(K3)
    steps_a(False)
    mixer()
    reduce(1, mixer_block, res.at[0], 3, 1.0)
    norm_to(res.at[1], 4)
    reduce(2, second, res.at[1], 5, 0.5)
    out_ref[...] = res[2]

    def done(copy):
        copy.wait_send()

    for k in range(nff + 1):
        def drain(s, carry):
            @pl.when(s <= z)
            def _():
                right(k, s, done)

            @pl.when(s >= z)
            def _():
                left(k, s, done)

            across(k, s, done)
            return carry

        lax.fori_loop(0, Z, drain, 0)
    across(K4, z, done)

    def drain_a(s, carry):
        @pl.when(s <= z)
        def _():
            right_a(s, done)

        @pl.when(s >= z)
        def _():
            left_a(s, done)

        return carry

    lax.fori_loop(0, Z, drain_a, 0)


def y_count(mesh):
    try:
        found = len({d.coords[1] for d in mesh.devices.reshape(-1)})
    except AttributeError:
        found = 1
    return found if found == 2 and mesh.shape["fs"] % 2 == 0 else 1


def solution(mesh):
    n_fs, n_tp = mesh.shape["fs"], mesh.shape["tp"]
    Y = y_count(mesh)
    Z, X = n_fs // Y, n_tp // 2

    def local(stream_in, norm_gains, gate, up, down, outer_w, inner_w, value_w, mixer_w, conv_taps):
        rows, width = stream_in.shape
        part, hid = gate.shape
        channels = outer_w.shape[1]
        shard = -(-part // 16) * 16
        Dp = n_fs * shard
        nff = 3 if hid % 384 == 0 else 1
        hc = hid // nff
        main = channels // 128 * 128
        rem = channels - main

        def widen(v):
            lead = v.shape[0]
            v = v.reshape(lead, n_fs, part)
            return jnp.pad(v, ((0, 0), (0, 0), (0, shard - part))).reshape(lead, Dp)

        sent = -(-part // 8) * 8

        def pack(w):
            return w if sent == part else jnp.pad(w, ((0, sent - part), (0, 0)))

        rest = [w[:, main:] for w in (outer_w, inner_w, value_w, mixer_w)]
        rest.append(jnp.zeros((part, 128 - 4 * rem), BF16))
        owns = [gate, up, down, outer_w, inner_w, value_w, mixer_w]
        owns = [pack(w) for w in owns + [jnp.concatenate(rest, axis=1)]]
        taps = lax.dynamic_slice_in_dim(
            conv_taps, lax.axis_index("tp") * channels, channels, 1
        ).astype(F32)
        taps = jnp.concatenate(
            [jnp.pad(taps[:, main:], ((0, 0), (3 * rem, 128 - 4 * rem))), taps[:, :main]], axis=1
        )
        half, quarter = rows // 2, rows // 4
        dma, vmem = pltpu.SemaphoreType.DMA, pltpu.VMEM
        out = pl.pallas_call(
            functools.partial(kernel, (Z, Y, X, shard, sent, width, hc, nff, main, rem)),
            out_shape=jax.ShapeDtypeStruct((rows, Dp), BF16),
            in_specs=[pl.BlockSpec(memory_space=pl.ANY)] * 8
            + [pl.BlockSpec(memory_space=pltpu.VMEM)] * 3,
            out_specs=pl.BlockSpec(memory_space=pltpu.VMEM),
            scratch_shapes=[
                vmem((nff, Dp, 3 * hc), BF16),
                vmem((Dp, 2 * main), BF16),
                vmem((Dp, 2 * main + 128), BF16),
                vmem((2, half, Dp), BF16),
                vmem((2, half, Dp), F32),
                vmem((2, half, main + 128), BF16),
                vmem((3, 2, quarter, Dp), BF16),
                vmem((3, 2, quarter, Dp), BF16),
                vmem((3, 2, quarter, Dp), BF16),
                vmem((3, 2, X - 1, quarter, Dp), BF16),
                vmem((3, rows, Dp), BF16),
                dma((3 * nff + 5,)),
                dma((nff + 2, 3, n_fs)),
                dma((nff + 2, n_fs)),
                dma((2, Z)),
                dma((Z,)),
                dma((2, 3, 2)),
                dma((3, 2, X - 1)),
                dma((3, 2, X - 1)),
                dma((2, 3, 2)),
            ],
            compiler_params=pltpu.CompilerParams(
                collective_id=0, has_side_effects=True, vmem_limit_bytes=60 * 1024 * 1024
            ),
        )(*owns, widen(stream_in), widen(norm_gains), taps)
        return out.reshape(rows, n_fs, shard)[:, :, :part].reshape(rows, width)

    return jax.shard_map(
        local,
        mesh=mesh,
        in_specs=(P("fs", None), P()) + (P("fs", "tp"),) * 7 + (P(),),
        out_specs=P("fs", None),
        check_vma=False,
    )
```

profile of v0, /device:TPU:0, one launch (start us, length us, event | category | flops | bytes accessed | tf_op | source)
XLA Modules:
  0.0 204.5 jit_solution(14010860139171708452)
XLA Ops:
  0.0 0.0 copy-start
  0.0 0.8 dynamic-slice_convert_fusion
  0.9 0.7 select_maximum_fusion.refs_10_
  1.5 0.9 slice.21
  2.4 0.9 slice.22
  3.3 0.9 slice.23
  4.2 0.9 slice.24
  5.1 0.8 concatenate.6.refs_7_
  5.9 1.0 reshape.20
  6.9 0.7 reshape.21.refs_9_
  7.6 0.0 copy-done
  7.6 0.1 pad.12
  7.7 1.5 copy.13.refs_8_
  9.2 192.6 %shard_map.100 = bf16[256,2176]{1,0:T(8,128)(2,1)} custom-call(bf16[264,768]{1,0:T(8,128)(2,1)} %refs_0_.1, bf16[264,768]{1,0:T(8,128)(2,1)} %refs_1_.1, bf16[264,768]{1,0:T(8,128)(2,1)} %refs_2_.1, bf16[264,264]{1,0:T(8,128)(2,1)} %refs_3_.1, bf16[264,264]{1,0:T(8,128)(2,1)} %refs_4_.1, bf16[264,264]{1,0:T(8,128)(2,1)} %refs_5_.1, ...), custom_call_target="tpu_custom_call" | custom-call | tf_op jit(solution)/shard_map/pallas_call | solution.py:443
  201.8 1.7 copy.14
  203.4 1.1 slice.30
  (4 shorter events, 0.0 us)
Async XLA Ops:
  0.0 7.6 %copy-start = (bf16[256,2112]{0,1:T(8,128)(2,1)S(1)}, bf16[256,2112]{0,1:T(8,128)(2,1)}, u32[]{:S(2)}) copy-start(bf16[256,2112]{0,1:T(8,128)(2,1)} %param.10) | copy-start | bytes 3244036
where the time goes:
time: 205 us; the launch traced here: 204 us
  Pallas kernels  193 us (94%)
  local copies, waits for them, and re-layouts  10.4 us (5%)
    pallas_call x1, Pallas kernels, local(): pl.pallas_call(functools.partial(kernel, (Z, Y, X, shard, sent, width, hc...  193 us

commit v1 on v0

--- a/solution.py
+++ b/solution.py
@@ -394,6 +394,648 @@
     lax.fori_loop(0, Z, drain_a, 0)
 
 
+def stream_kernel(cfg, *refs):
+    Z, shard, part, width, hc, nff, main, rem, grp = cfg
+    own_refs = refs[:7]
+    stream_ref, gains_ref, taps_ref, out_ref = refs[7:11]
+    (ff, g3, gv, gb, pr, edge, xt, gtmp, gcol, gains, tbuf, normed, hid, mixed,
+     part_buf, crecv, xsend, xrecv, tot, res,
+     lsem, zsend, recv, psend, precv, pysend, pyrecv, csem, xsem, tsem, osem) = refs[11:]
+    Y = 2
+    n_fs = Z * Y
+    rows = normed.shape[0]
+    Dp = n_fs * shard
+    groups = 128 // 32
+    pair = Y * shard
+    last, K3, KB = nff - 1, nff, nff + 1
+    f, t = lax.axis_index("fs"), lax.axis_index("tp")
+    z, y = f // Y, f % Y
+    c, x = t % 2, t // 2
+    core_peer = (f, x * 2 + 1 - c)
+    x_peer = (f, (1 - x) * 2 + c)
+    dev_y = (z * Y + (1 - y), t)
+
+    def dev_z(zz):
+        return (zz * Y + y, t)
+
+    own_row = pl.multiple_of(f * shard, 16)
+    here = pl.ds(own_row, part)
+    lead = pl.ds(0, main)
+    gate, up, down, ow, iw, vw, mw = own_refs
+    moves = []
+    for k in range(nff):
+        for j, w in enumerate((gate, up, down)):
+            moves.append((k, w.at[:, pl.ds(k * hc, hc)], ff.at[k, here, pl.ds(j * hc, hc)]))
+    moves.append((K3, ow.at[:, lead], g3.at[here, lead]))
+    moves.append((K3, iw.at[:, lead], g3.at[here, pl.ds(main, main)]))
+    moves.append((K3, vw.at[:, lead], gv.at[here, lead]))
+    moves.append((K3, mw.at[:, lead], gb.at[here, :]))
+    for j, w in enumerate((ow, iw, vw, mw)):
+        moves.append((nff + 1, w, edge.at[j]))
+    for s in range(n_fs):
+        moves.append((nff + 2, stream_ref.at[pl.ds(s * part, part)], xt.at[pl.ds(s * shard, part)]))
+    local = [
+        (k, pltpu.make_async_copy(src, dst, lsem.at[n])) for n, (k, src, dst) in enumerate(moves)
+    ]
+
+    for s in range(n_fs):
+        tail = pl.ds(s * shard + shard - 16, 16)
+        for k in range(nff):
+            ff[k, tail] = jnp.zeros((16, 3 * hc), BF16)
+        g3[tail] = jnp.zeros((16, 2 * main), BF16)
+        gv[tail] = jnp.zeros((16, main + 128), BF16)
+        gb[tail] = jnp.zeros((16, main), BF16)
+        xt[tail] = jnp.zeros((16, rows), BF16)
+
+    barrier = pltpu.get_barrier_semaphore()
+
+    def greet(d):
+        pl.semaphore_signal(barrier, inc=1, device_id=d, device_id_type=MESH)
+
+    for d in (core_peer, x_peer, dev_y):
+        greet(d)
+
+    @pl.when(z > 0)
+    def _():
+        greet(dev_z(z - 1))
+
+    @pl.when(z < Z - 1)
+    def _():
+        greet(dev_z(z + 1))
+
+    for _, copy in local:
+        copy.start()
+    peers = 3 + (z > 0).astype(jnp.int32) + (z < Z - 1).astype(jnp.int32)
+    pl.semaphore_wait(barrier, peers)
+
+    def local_wait(k):
+        for owner, copy in local:
+            if owner == k:
+                copy.wait()
+
+    def remote(k, s, way, d):
+        at = pl.ds(pl.multiple_of(s * shard, 16), part)
+        if k < last:
+            ref = ff.at[k, at]
+        elif k == last:
+            ref = ff.at[k, at, 0 : 2 * hc]
+        else:
+            ref = (g3 if k == K3 else gb).at[at]
+        return pltpu.make_async_remote_copy(
+            src_ref=ref, dst_ref=ref, send_sem=zsend.at[k, way, s], recv_sem=recv.at[k, s],
+            device_id=d, device_id_type=MESH,
+        )
+
+    def right(k, s, act):
+        @pl.when(z < Z - 1)
+        def _():
+            act(remote(k, s * Y + y, 0, dev_z(z + 1)))
+
+    def left(k, s, act):
+        @pl.when(z > 0)
+        def _():
+            act(remote(k, s * Y + y, 1, dev_z(z - 1)))
+
+    def across(k, s, act):
+        act(remote(k, s * Y + y, 2, dev_y))
+
+    def go(copy):
+        copy.start()
+
+    def own_z(k):
+        right(k, z, go)
+        left(k, z, go)
+
+    def own_y(k):
+        across(k, z, go)
+
+    at_end = (z == 0) | (z == Z - 1)
+
+    def zsteps(k):
+        def step(i, carry):
+            @pl.when(z - 1 - i >= 0)
+            def _():
+                s = z - 1 - i
+                remote(k, s * Y + y, 0, dev_z(z - 1)).wait_recv()
+                right(k, s, go)
+                across(k, s, go)
+
+            @pl.when(z + 1 + i < Z)
+            def _():
+                s = z + 1 + i
+                remote(k, s * Y + y, 0, dev_z(z + 1)).wait_recv()
+                left(k, s, go)
+                across(k, s, go)
+
+            return carry
+
+        lax.fori_loop(0, Z - 1, step, 0)
+
+    def wait_across(k):
+        def step(s, carry):
+            remote(k, s * Y + 1 - y, 2, dev_y).wait_recv()
+            return carry
+
+        lax.fori_loop(0, Z, step, 0)
+
+    def piece(q, first, count):
+        if q == 2:
+            return pr.at[pl.ds(pl.multiple_of(first * grp, 16), count * grp)]
+        at = pl.ds(pl.multiple_of(first * shard, 16), (count - 1) * shard + part)
+        return gv.at[at, lead] if q == 1 else ff.at[last, at, 2 * hc : 3 * hc]
+
+    def across_p(q, s):
+        ref = piece(q, s, 1)
+        return pltpu.make_async_remote_copy(
+            src_ref=ref, dst_ref=ref, send_sem=pysend.at[q], recv_sem=pyrecv.at[q],
+            device_id=dev_y, device_id_type=MESH,
+        )
+
+    def remote_p(q, s, way, d):
+        ref = piece(q, s * Y, Y)
+        return pltpu.make_async_remote_copy(
+            src_ref=ref, dst_ref=ref, send_sem=psend.at[q, way, s], recv_sem=precv.at[q, s],
+            device_id=d, device_id_type=MESH,
+        )
+
+    def right_p(q, s, act):
+        @pl.when(z < Z - 1)
+        def _():
+            act(remote_p(q, s, 0, dev_z(z + 1)))
+
+    def left_p(q, s, act):
+        @pl.when(z > 0)
+        def _():
+            act(remote_p(q, s, 1, dev_z(z - 1)))
+
+    def start_p(q):
+        across_p(q, z * Y + 1 - y).wait_recv()
+        right_p(q, z, go)
+        left_p(q, z, go)
+
+    def steps_p(qs, forward):
+        def step(i, carry):
+            @pl.when((z - 1 - i >= 0) & ((z < Z - 1) if forward else (z == Z - 1)))
+            def _():
+                s = z - 1 - i
+                for q in qs:
+                    remote_p(q, s, 0, dev_z(z - 1)).wait_recv()
+                    if forward:
+                        right_p(q, s, go)
+
+            @pl.when((z + 1 + i < Z) & ((z > 0) if forward else (z == 0)))
+            def _():
+                s = z + 1 + i
+                for q in qs:
+                    remote_p(q, s, 0, dev_z(z + 1)).wait_recv()
+                    if forward:
+                        left_p(q, s, go)
+
+            return carry
+
+        lax.fori_loop(0, Z - 1, step, 0)
+
+    def pack_edges():
+        packed = jnp.zeros((grp, 128), F32)
+        for j in range(groups):
+            count = min(grp, part - j * grp)
+            if count <= 0:
+                continue
+            block = jnp.zeros((count, 128), F32)
+            row = lax.broadcasted_iota(jnp.int32, (rem, 128), 0)
+            lane = lax.broadcasted_iota(jnp.int32, (rem, 128), 1)
+            for k in range(4):
+                place = jnp.where(lane == row + (32 * j + rem * k), 1.0, 0.0).astype(BF16)
+                source = edge[k, j * grp : j * grp + count, main : main + rem]
+                block = block + jnp.dot(source, place, preferred_element_type=F32)
+            if count < grp:
+                block = jnp.concatenate([block, jnp.zeros((grp - count, 128), F32)], axis=0)
+            packed = packed + block
+        pr[pl.ds(pl.multiple_of(f * grp, 16), grp)] = packed.astype(BF16)
+
+    def unpack_edges():
+        row = lax.broadcasted_iota(jnp.int32, (128, 128), 0)
+        lane = lax.broadcasted_iota(jnp.int32, (128, 128), 1)
+
+        def body(s, carry):
+            packed = pr[pl.ds(pl.multiple_of(s * grp, 16), grp)]
+            for j in range(groups):
+                count = min(grp, shard - j * grp)
+                if count <= 0:
+                    continue
+                pick = jnp.where((lane < 32) & (row == lane + 32 * j), 1.0, 0.0).astype(BF16)
+                block = jnp.dot(packed, pick, preferred_element_type=F32)[:count]
+                at = pl.ds(pl.multiple_of(s * shard + j * grp, 16), count)
+                gv[at, main : main + 128] = block.astype(BF16)
+            return carry
+
+        lax.fori_loop(0, n_fs, body, 0)
+
+    def prepare_gains():
+        gtmp[...] = jnp.zeros(gtmp.shape, F32)
+        gtmp[0:6, 0:width] = gains_ref[...]
+        for i in range(gtmp.shape[1] // 128):
+            gcol[i * 128 : (i + 1) * 128] = gtmp[:, i * 128 : (i + 1) * 128].T
+
+        def body(s, carry):
+            for j in range(6):
+                column = gcol[pl.ds(pl.multiple_of(s * part, 8), part), j : j + 1]
+                at = pl.ds(pl.multiple_of(s * shard, 16), part)
+                gains[j, at] = jnp.broadcast_to(column, (part, 128))
+                pad = pl.ds(pl.multiple_of(s * shard + part, 8), shard - part)
+                gains[j, pad] = jnp.zeros((shard - part, 128), F32)
+            return carry
+
+        lax.fori_loop(0, n_fs, body, 0)
+
+    def prepare_taps():
+        n_tp = lax.axis_size("tp")
+        channels = taps_ref.shape[1] // n_tp
+        lanes = tbuf.shape[1]
+        tbuf[...] = jnp.zeros(tbuf.shape, F32)
+        tbuf[0:CONV_K, 0 : taps_ref.shape[1]] = taps_ref[...].astype(F32)
+        full = tbuf[...]
+        mine = full
+        for i in range(1, n_tp):
+            mine = jnp.where(t == i, pltpu.roll(full, lanes - channels * i, 1), mine)
+        tbuf[:, 0:main] = mine[:, 0:main]
+        rest = pltpu.roll(mine[:, main : main + 128], 3 * rem, 1)
+        lane = lax.broadcasted_iota(jnp.int32, rest.shape, 1)
+        tbuf[:, main : main + 128] = jnp.where((lane >= 3 * rem) & (lane < 4 * rem), rest, 0.0)
+
+    BLK = 128
+    nblk = Dp // BLK
+
+    def squares(v):
+        return jnp.sum((v * v).reshape(BLK // 8, 8, rows), axis=0)
+
+    def block_at(i):
+        return pl.ds(pl.multiple_of(i * BLK, BLK), BLK)
+
+    def inverse(sums):
+        return lax.rsqrt(jnp.sum(sums, axis=0, keepdims=True) * (1.0 / width) + EPSILON)
+
+    def gain_block(row, at):
+        g = gains[row, at]
+        return jnp.concatenate([g] * (rows // 128), axis=1)
+
+    def sum_squares(source):
+        def body(i, sums):
+            return sums + squares(source[block_at(i)].astype(F32))
+
+        return lax.fori_loop(0, nblk, body, jnp.zeros((8, rows), F32))
+
+    def norm_to(source, sums, row):
+        scale = inverse(sums)
+
+        def body(i, carry):
+            at = block_at(i)
+            v = source[at].astype(F32) * scale * gain_block(row, at)
+            normed[:, at] = v.T.astype(BF16)
+            return carry
+
+        lax.fori_loop(0, nblk, body, 0)
+
+    def update(r, source, row, factor):
+        scale = inverse(sum_squares(tot.at[r])) * factor
+
+        def body(i, sums):
+            at = block_at(i)
+            v = source[at].astype(F32) + tot[r, at].astype(F32) * scale * gain_block(row, at)
+            v = v.astype(BF16)
+            res[r, at] = v
+            return sums + squares(v.astype(F32))
+
+        return lax.fori_loop(0, nblk, body, jnp.zeros((8, rows), F32))
+
+    def hidden(k):
+        n = normed[...]
+        gate_v = jnp.dot(n, ff[k, :, 0:hc], preferred_element_type=F32)
+        up_v = jnp.dot(n, ff[k, :, hc : 2 * hc], preferred_element_type=F32)
+        hid[k] = (gate_v / (1.0 + jnp.exp(-gate_v)) * up_v).astype(BF16)
+
+    def pair_at(j):
+        return pl.ds(pl.multiple_of(j * pair, 16), pair)
+
+    def ffn_pair(r, j):
+        at = pair_at(j)
+        total = lax.dot_general(ff[0, at, 2 * hc :], hid[0], NT, preferred_element_type=F32)
+        for k in range(1, nff):
+            total = total + lax.dot_general(
+                ff[k, at, 2 * hc :], hid[k], NT, preferred_element_type=F32
+            )
+        part_buf[r, j] = total.astype(BF16)
+
+    def mixer_pair(r, j):
+        remote(KB, j * Y + 1 - y, 2, dev_y).wait_recv()
+        at = pair_at(j)
+        total = lax.dot_general(gb[at], mixed[:, 0:main], NT, preferred_element_type=F32)
+        total = total + lax.dot_general(
+            gv[at, main : main + 128], mixed[:, main:], NT, preferred_element_type=F32
+        )
+        part_buf[r, j] = total.astype(BF16)
+
+    mine = pl.ds(pl.multiple_of(c * shard, 16), shard)
+    other = pl.ds(pl.multiple_of((1 - c) * shard, 16), shard)
+
+    def core_copy(r, j):
+        return pltpu.make_async_remote_copy(
+            src_ref=part_buf.at[r, j, other], dst_ref=crecv.at[r, j], send_sem=csem.at[0, r, j],
+            recv_sem=csem.at[1, r, j], device_id=core_peer, device_id_type=MESH,
+        )
+
+    def x_copy(r, j):
+        return pltpu.make_async_remote_copy(
+            src_ref=xsend.at[r, j], dst_ref=xrecv.at[r, j], send_sem=xsem.at[0, r, j],
+            recv_sem=xsem.at[1, r, j], device_id=x_peer, device_id_type=MESH,
+        )
+
+    def tot_copy(r, j):
+        at = pl.ds(pl.multiple_of(j * pair + c * shard, 16), shard)
+        return pltpu.make_async_remote_copy(
+            src_ref=tot.at[r, at], dst_ref=tot.at[r, at], send_sem=tsem.at[0, r, j],
+            recv_sem=tsem.at[1, r, j], device_id=core_peer, device_id_type=MESH,
+        )
+
+    near = jnp.minimum(z, Z - 1 - z)
+    low = z <= Z - 1 - z
+
+    def order(s):
+        step = (s + 1) // 2
+        close = jnp.where(s % 2 == 1, z - step, z + step)
+        return jnp.where(s <= 2 * near, close, jnp.where(low, s, Z - 1 - s))
+
+    def pass_on(j):
+        remote(KB, j * Y + y, 0, dev_z(jnp.where(z == 0, z + 1, z - 1))).wait_recv()
+        across(KB, j, go)
+
+    def reduce(r, compute):
+        def cross(j):
+            core_copy(r, j).wait_recv()
+            xsend[r, j] = (
+                part_buf[r, j, mine].astype(F32) + crecv[r, j].astype(F32)
+            ).astype(BF16)
+            x_copy(r, j).start()
+
+        def send(s, carry):
+            j = order(s)
+            if r == 1:
+                @pl.when(at_end & (s < Z - 1))
+                def _():
+                    pass_on(order(s + 1))
+
+            compute(r, j)
+            core_copy(r, j).start()
+
+            @pl.when(s > 0)
+            def _():
+                cross(order(s - 1))
+
+            return carry
+
+        def receive(s, carry):
+            j = order(s)
+            x_copy(r, j).wait_recv()
+            at = pl.ds(pl.multiple_of(j * pair + c * shard, 16), shard)
+            tot[r, at] = (xsend[r, j].astype(F32) + xrecv[r, j].astype(F32)).astype(BF16)
+            tot_copy(r, j).start()
+            return carry
+
+        def finish(s, carry):
+            tot_copy(r, order(s)).wait_recv()
+            return carry
+
+        lax.fori_loop(0, Z, send, 0)
+        cross(order(Z - 1))
+        lax.fori_loop(0, Z, receive, 0)
+        lax.fori_loop(0, Z, finish, 0)
+
+    def mixer():
+        n = normed[...]
+        outer_inner = jnp.dot(n, g3[...], preferred_element_type=F32)
+        outer_inner = outer_inner.astype(BF16).astype(F32)
+        value_rest = jnp.dot(n, gv[...], preferred_element_type=F32)
+        value_rest = value_rest.astype(BF16).astype(F32)
+        rest = value_rest[:, main:]
+        lane = lax.broadcasted_iota(jnp.int32, rest.shape, 1)
+        keep = (lane >= 3 * rem) & (lane < 4 * rem)
+        rests = [jnp.where(keep, pltpu.roll(rest, (3 - j) * rem, 1), 0.0) for j in range(3)]
+        parts = [
+            (outer_inner[:, 0:main], outer_inner[:, main:], value_rest[:, 0:main], 0),
+            (rests[0], rests[1], rests[2], main),
+        ]
+        for outer, inner, value, first in parts:
+            lanes = outer.shape[1]
+            gated = inner * value
+            token = lax.broadcasted_iota(jnp.int32, gated.shape, 0)
+            conv = jnp.zeros_like(gated)
+            for j in range(CONV_K):
+                back = CONV_K - 1 - j
+                moved = gated
+                if back:
+                    moved = jnp.where(token >= back, pltpu.roll(gated, back, 0), 0.0)
+                conv = conv + tbuf[j : j + 1, first : first + lanes] * moved
+            mixed[:, first : first + lanes] = (outer * conv).astype(BF16)
+
+    for k in range(2):
+        local_wait(k)
+        own_z(k)
+        own_y(k)
+    local_wait(nff + 1)
+    pack_edges()
+    for k in range(2, nff + 1):
+        local_wait(k)
+    for q in range(3):
+        across_p(q, f).start()
+
+    @pl.when(at_end)
+    def _():
+        for k in range(2, KB + 1):
+            own_z(k)
+
+    local_wait(nff + 2)
+    prepare_gains()
+    prepare_taps()
+    norm_to(xt, sum_squares(xt), 0)
+    zsteps(0)
+
+    @pl.when(at_end)
+    def _():
+        for q in range(3):
+            start_p(q)
+
+    @pl.when(~at_end)
+    def _():
+        own_z(2)
+
+    own_y(2)
+    for k in range(1, last):
+        zsteps(k)
+        wait_across(k - 1)
+        hidden(k - 1)
+    zsteps(last)
+
+    @pl.when(~at_end)
+    def _():
+        start_p(0)
+        steps_p((0,), True)
+        own_z(K3)
+
+    own_y(K3)
+    wait_across(last - 1)
+    hidden(last - 1)
+    zsteps(K3)
+
+    @pl.when(~at_end)
+    def _():
+        start_p(1)
+        start_p(2)
+        steps_p((1, 2), True)
+        own_z(KB)
+
+    own_y(KB)
+
+    @pl.when(~at_end)
+    def _():
+        zsteps(KB)
+
+    wait_across(last)
+    steps_p((0,), False)
+    hidden(last)
+    reduce(0, ffn_pair)
+    norm_to(res.at[0], update(0, xt, 1, 0.5), 2)
+    wait_across(K3)
+    steps_p((1, 2), False)
+    unpack_edges()
+    mixer()
+    reduce(1, mixer_pair)
+    norm_to(res.at[1], update(1, res.at[0], 3, 1.0), 4)
+
+    def again(k, carry):
+        hidden(k)
+        return carry
+
+    lax.fori_loop(0, nff, again, 0)
+    reduce(2, ffn_pair)
+    update(2, res.at[1], 5, 0.5)
+    outs = [
+        pltpu.make_async_copy(
+            res.at[2, pl.ds(s * shard, part)], out_ref.at[pl.ds(s * part, part)], osem.at[s]
+        )
+        for s in range(n_fs)
+    ]
+    for copy in outs:
+        copy.start()
+
+    def done(copy):
+        copy.wait_send()
+
+    for k in range(nff + 2):
+        def drain(s, carry):
+            @pl.when(s <= z)
+            def _():
+                right(k, s, done)
+
+            @pl.when(s >= z)
+            def _():
+                left(k, s, done)
+
+            across(k, s, done)
+            return carry
+
+        lax.fori_loop(0, Z, drain, 0)
+    for q in range(3):
+        across_p(q, f).wait_send()
+
+        def drain_p(s, carry):
+            @pl.when(s <= z)
+            def _():
+                right_p(q, s, done)
+
+            @pl.when(s >= z)
+            def _():
+                left_p(q, s, done)
+
+            return carry
+
+        lax.fori_loop(0, Z, drain_p, 0)
+
+    for r in range(3):
+        def drain_r(s, carry):
+            core_copy(r, s).wait_send()
+            x_copy(r, s).wait_send()
+            tot_copy(r, s).wait_send()
+            return carry
+
+        lax.fori_loop(0, Z, drain_r, 0)
+    for copy in outs:
+        copy.wait()
+
+
+def stream_form(mesh, Z):
+    def local(stream_in, norm_gains, gate, up, down, outer_w, inner_w, value_w, mixer_w, conv_taps):
+        rows, width = stream_in.shape
+        part, hid = gate.shape
+        channels = outer_w.shape[1]
+        n_fs = 2 * Z
+        shard = -(-part // 16) * 16
+        Dp = n_fs * shard
+        nff = 3
+        hc = hid // nff
+        main = channels // 128 * 128
+        rem = channels - main
+        grp = -(-part // 64) * 16
+        lanes = -(-width // 128) * 128
+        taps = -(-conv_taps.shape[1] // 128) * 128
+        dma, vmem = pltpu.SemaphoreType.DMA, pltpu.VMEM
+        out = pl.pallas_call(
+            functools.partial(stream_kernel, (Z, shard, part, width, hc, nff, main, rem, grp)),
+            out_shape=jax.ShapeDtypeStruct((width, rows), BF16),
+            in_specs=[pl.BlockSpec(memory_space=pl.ANY)] * 8
+            + [pl.BlockSpec(memory_space=pltpu.VMEM)] * 2,
+            out_specs=pl.BlockSpec(memory_space=pl.ANY),
+            scratch_shapes=[
+                vmem((nff, Dp, 3 * hc), BF16),
+                vmem((Dp, 2 * main), BF16),
+                vmem((Dp, main + 128), BF16),
+                vmem((Dp, main), BF16),
+                vmem((n_fs * grp, 128), BF16),
+                vmem((4, part, channels), BF16),
+                vmem((Dp, rows), BF16),
+                vmem((128, lanes), F32),
+                vmem((lanes, 128), F32),
+                vmem((6, Dp, 128), F32),
+                vmem((8, taps), F32),
+                vmem((rows, Dp), BF16),
+                vmem((nff, rows, hc), BF16),
+                vmem((rows, main + 128), BF16),
+                vmem((3, Z, 2 * shard, rows), BF16),
+                vmem((3, Z, shard, rows), BF16),
+                vmem((3, Z, shard, rows), BF16),
+                vmem((3, Z, shard, rows), BF16),
+                vmem((3, Dp, rows), BF16),
+                vmem((3, Dp, rows), BF16),
+                dma((3 * nff + 8 + n_fs,)),
+                dma((nff + 2, 3, n_fs)),
+                dma((nff + 2, n_fs)),
+                dma((3, 2, Z)),
+                dma((3, Z)),
+                dma((3,)),
+                dma((3,)),
+                dma((2, 3, Z)),
+                dma((2, 3, Z)),
+                dma((2, 3, Z)),
+                dma((n_fs,)),
+            ],
+            compiler_params=pltpu.CompilerParams(
+                collective_id=0, has_side_effects=True, vmem_limit_bytes=60 * 1024 * 1024
+            ),
+        )(gate, up, down, outer_w, inner_w, value_w, mixer_w, stream_in.T, norm_gains, conv_taps)
+        return out.T
+
+    return local
+
+
 def y_count(mesh):
     try:
         found = len({d.coords[1] for d in mesh.devices.reshape(-1)})
@@ -407,7 +1049,7 @@
     Y = y_count(mesh)
     Z, X = n_fs // Y, n_tp // 2
 
-    def local(stream_in, norm_gains, gate, up, down, outer_w, inner_w, value_w, mixer_w, conv_taps):
+    def chain_form(stream_in, norm_gains, gate, up, down, outer_w, inner_w, value_w, mixer_w, conv_taps):
         rows, width = stream_in.shape
         part, hid = gate.shape
         channels = outer_w.shape[1]
@@ -474,6 +1116,15 @@
         )(*owns, widen(stream_in), widen(norm_gains), taps)
         return out.reshape(rows, n_fs, shard)[:, :, :part].reshape(rows, width)
 
+    def local(*args):
+        rows, width = args[0].shape
+        part, channels = args[5].shape
+        rem = channels % 128
+        fits = Y == 2 and X == 2 and part % 8 == 0 and 0 < rem <= 8 and rows % 128 == 0
+        fits = fits and (n_fs * (-(-part // 16) * 16)) % 128 == 0 and channels > 128
+        fits = fits and args[2].shape[1] % 384 == 0 and Z > 2
+        return (stream_form(mesh, Z) if fits else chain_form)(*args)
+
     return jax.shard_map(
         local,
         mesh=mesh,

time: 205 us -> 187 us (0.912)
  Pallas kernels: 193 us -> 183 us
  local copies, waits for them, and re-layouts: 10.4 us -> 2.29 us
    pallas_call x1, Pallas kernels: 193 us -> 183 us  [local(): pl.pallas_call(functools.partial(stream_kernel, (Z, shard, part, width, h...]
    slice x7 -> x0, local copies, waits for them, and re-layouts: 4.6 us -> none  [the longest x4 3.55 us: local(): rest = [w[:, main:] for w in (outer_w, inner_w, value_w, mixer_w)]]
    reshape x3 -> x0, local copies, waits for them, and re-layouts: 3.22 us -> none  [the longest x2 2.25 us: widen(): return jnp.pad(v, ((0, 0), (0, 0), (0, shard - part))).reshape(lead, Dp)]
    unnamed x2 -> x1, local copies, waits for them, and re-layouts: 0.01 us -> 2.29 us
where the time goes in v1:
time: 187 us; the launch traced here: 185 us
  Pallas kernels  183 us (98%)
  local copies, waits for them, and re-layouts  2.29 us (1%)
    pallas_call x1, Pallas kernels, local(): pl.pallas_call(functools.partial(stream_kernel, (Z, shard, part, width, h...  183 us

profile of v1, /device:TPU:0, one launch (start us, length us, event | category | flops | bytes accessed | tf_op | source)
XLA Modules:
  0.0 184.8 jit_solution(9260724710050663884)
XLA Ops:
  0.0 182.5 %shard_map.100 = bf16[2112,256]{1,0:T(8,128)(2,1)} custom-call(bf16[264,768]{1,0:T(8,128)(2,1)} %refs_0_.1, bf16[264,768]{1,0:T(8,128)(2,1)} %refs_1_.1, bf16[264,768]{1,0:T(8,128)(2,1)} %refs_2_.1, bf16[264,264]{1,0:T(8,128)(2,1)} %refs_3_.1, bf16[264,264]{1,0:T(8,128)(2,1)} %refs_4_.1, bf16[264,264]{1,0:T(8,128)(2,1)} %refs_5_.1, ...), custom_call_target="tpu_custom_call" | custom-call | tf_op jit(solution)/shard_map/pallas_call | solution.py:991
  182.5 2.3 %copy.12 = bf16[256,2112]{0,1:T(8,128)(2,1)} copy(bf16[256,2112]{0,1:T(8,128)(2,1)} %bitcast.2) | data formatting | bytes 2162688

commit v2 on v1

--- a/solution.py
+++ b/solution.py
@@ -438,15 +438,19 @@
         (k, pltpu.make_async_copy(src, dst, lsem.at[n])) for n, (k, src, dst) in enumerate(moves)
     ]
 
-    for s in range(n_fs):
-        tail = pl.ds(s * shard + shard - 16, 16)
-        for k in range(nff):
-            ff[k, tail] = jnp.zeros((16, 3 * hc), BF16)
-        g3[tail] = jnp.zeros((16, 2 * main), BF16)
-        gv[tail] = jnp.zeros((16, main + 128), BF16)
-        gb[tail] = jnp.zeros((16, main), BF16)
-        xt[tail] = jnp.zeros((16, rows), BF16)
-
+    def clear_pads():
+        for s in range(n_fs):
+            pad = pl.ds(s * shard + part, shard - part)
+            for k in range(nff):
+                ff[k, pad] = jnp.zeros((shard - part, 3 * hc), BF16)
+            g3[pad] = jnp.zeros((shard - part, 2 * main), BF16)
+            gv[pad] = jnp.zeros((shard - part, main + 128), BF16)
+            gb[pad] = jnp.zeros((shard - part, main), BF16)
+            xt[pad] = jnp.zeros((shard - part, rows), BF16)
+
+    for _, copy in local:
+        copy.start()
+    clear_pads()
     barrier = pltpu.get_barrier_semaphore()
 
     def greet(d):
@@ -463,8 +467,6 @@
     def _():
         greet(dev_z(z + 1))
 
-    for _, copy in local:
-        copy.start()
     peers = 3 + (z > 0).astype(jnp.int32) + (z < Z - 1).astype(jnp.int32)
     pl.semaphore_wait(barrier, peers)
 
@@ -502,14 +504,27 @@
     def go(copy):
         copy.start()
 
-    def own_z(k):
-        right(k, z, go)
-        left(k, z, go)
+    near = jnp.minimum(z, Z - 1 - z)
+    low = z <= Z - 1 - z
+    at_end = (z == 0) | (z == Z - 1)
+
+    def inward(go_right, go_left):
+        @pl.when(low)
+        def _():
+            go_right()
+
+        @pl.when(~low)
+        def _():
+            go_left()
+
+    def own_in(k):
+        inward(lambda: right(k, z, go), lambda: left(k, z, go))
+
+    def own_out(k):
+        inward(lambda: left(k, z, go), lambda: right(k, z, go))
 
     def own_y(k):
         across(k, z, go)
-
-    at_end = (z == 0) | (z == Z - 1)
 
     def zsteps(k):
         def step(i, carry):
@@ -542,6 +557,8 @@
         if q == 2:
             return pr.at[pl.ds(pl.multiple_of(first * grp, 16), count * grp)]
         at = pl.ds(pl.multiple_of(first * shard, 16), (count - 1) * shard + part)
+        if q == 3:
+            return gb.at[at]
         return gv.at[at, lead] if q == 1 else ff.at[last, at, 2 * hc : 3 * hc]
 
     def across_p(q, s):
@@ -568,10 +585,12 @@
         def _():
             act(remote_p(q, s, 1, dev_z(z - 1)))
 
-    def start_p(q):
+    def start_in(q):
         across_p(q, z * Y + 1 - y).wait_recv()
-        right_p(q, z, go)
-        left_p(q, z, go)
+        inward(lambda: right_p(q, z, go), lambda: left_p(q, z, go))
+
+    def start_out(q):
+        inward(lambda: left_p(q, z, go), lambda: right_p(q, z, go))
 
     def steps_p(qs, forward):
         def step(i, carry):
@@ -590,6 +609,45 @@
                     remote_p(q, s, 0, dev_z(z + 1)).wait_recv()
                     if forward:
                         left_p(q, s, go)
+
+            return carry
+
+        lax.fori_loop(0, Z - 1, step, 0)
+
+    def inside(s):
+        return (s > 0) & (s < Z - 1)
+
+    def steps_b():
+        def step(i, carry):
+            @pl.when(z - 1 - i >= 0)
+            def _():
+                s = z - 1 - i
+
+                @pl.when(s > 0)
+                def _():
+                    remote(KB, s * Y + y, 0, dev_z(z - 1)).wait_recv()
+                    right(KB, s, go)
+                    across(KB, s, go)
+
+                @pl.when(s == 0)
+                def _():
+                    remote_p(3, s, 0, dev_z(z - 1)).wait_recv()
+                    right_p(3, s, go)
+
+            @pl.when(z + 1 + i < Z)
+            def _():
+                s = z + 1 + i
+
+                @pl.when(s < Z - 1)
+                def _():
+                    remote(KB, s * Y + y, 0, dev_z(z + 1)).wait_recv()
+                    left(KB, s, go)
+                    across(KB, s, go)
+
+                @pl.when(s == Z - 1)
+                def _():
+                    remote_p(3, s, 0, dev_z(z + 1)).wait_recv()
+                    left_p(3, s, go)
 
             return carry
 
@@ -727,7 +785,10 @@
         part_buf[r, j] = total.astype(BF16)
 
     def mixer_pair(r, j):
-        remote(KB, j * Y + 1 - y, 2, dev_y).wait_recv()
+        @pl.when(inside(j))
+        def _():
+            remote(KB, j * Y + 1 - y, 2, dev_y).wait_recv()
+
         at = pair_at(j)
         total = lax.dot_general(gb[at], mixed[:, 0:main], NT, preferred_element_type=F32)
         total = total + lax.dot_general(
@@ -757,19 +818,37 @@
             recv_sem=tsem.at[1, r, j], device_id=core_peer, device_id_type=MESH,
         )
 
-    near = jnp.minimum(z, Z - 1 - z)
-    low = z <= Z - 1 - z
-
     def order(s):
         step = (s + 1) // 2
         close = jnp.where(s % 2 == 1, z - step, z + step)
         return jnp.where(s <= 2 * near, close, jnp.where(low, s, Z - 1 - s))
 
     def pass_on(j):
-        remote(KB, j * Y + y, 0, dev_z(jnp.where(z == 0, z + 1, z - 1))).wait_recv()
-        across(KB, j, go)
-
-    def reduce(r, compute):
+        source = dev_z(jnp.where(z == 0, z + 1, z - 1))
+
+        @pl.when(inside(j))
+        def _():
+            remote(KB, j * Y + y, 0, source).wait_recv()
+            across(KB, j, go)
+
+        @pl.when(~inside(j))
+        def _():
+            remote_p(3, j, 0, source).wait_recv()
+
+    def end_steps(first, stop):
+        source = dev_z(jnp.where(z == 0, z + 1, z - 1))
+
+        def step(s, carry):
+            j = order(s)
+            remote(K3, j * Y + y, 0, source).wait_recv()
+            across(K3, j, go)
+            return carry
+
+        @pl.when(at_end)
+        def _():
+            lax.fori_loop(first, stop, step, 0)
+
+    def reduce(r, compute, hooks):
         def cross(j):
             core_copy(r, j).wait_recv()
             xsend[r, j] = (
@@ -807,7 +886,12 @@
 
         lax.fori_loop(0, Z, send, 0)
         cross(order(Z - 1))
-        lax.fori_loop(0, Z, receive, 0)
+        if hooks:
+            hooks[0]()
+        lax.fori_loop(0, Z // 2, receive, 0)
+        if hooks:
+            hooks[1]()
+        lax.fori_loop(Z // 2, Z, receive, 0)
         lax.fori_loop(0, Z, finish, 0)
 
     def mixer():
@@ -839,7 +923,8 @@
 
     for k in range(2):
         local_wait(k)
-        own_z(k)
+        own_in(k)
+        own_out(k)
         own_y(k)
     local_wait(nff + 1)
     pack_edges()
@@ -847,68 +932,71 @@
         local_wait(k)
     for q in range(3):
         across_p(q, f).start()
-
     @pl.when(at_end)
     def _():
-        for k in range(2, KB + 1):
-            own_z(k)
-
+        across_p(3, f).start()
+        for k in range(2, K3 + 1):
+            own_in(k)
+
+    own_out(2)
+    own_y(2)
     local_wait(nff + 2)
     prepare_gains()
     prepare_taps()
     norm_to(xt, sum_squares(xt), 0)
     zsteps(0)
 
+    @pl.when(~at_end)
+    def _():
+        own_in(2)
+
+    start_in(0)
+    start_out(0)
+
     @pl.when(at_end)
     def _():
-        for q in range(3):
-            start_p(q)
+        for q in range(1, 4):
+            start_in(q)
+
+    zsteps(1)
+    own_out(K3)
 
     @pl.when(~at_end)
     def _():
-        own_z(2)
-
-    own_y(2)
-    for k in range(1, last):
-        zsteps(k)
-        wait_across(k - 1)
-        hidden(k - 1)
+        own_in(K3)
+        start_in(1)
+        start_in(2)
+        own_in(KB)
+
+    wait_across(0)
+    hidden(0)
     zsteps(last)
+    steps_p((0,), True)
+    own_y(K3)
 
     @pl.when(~at_end)
     def _():
-        start_p(0)
-        steps_p((0,), True)
-        own_z(K3)
-
-    own_y(K3)
-    wait_across(last - 1)
-    hidden(last - 1)
-    zsteps(K3)
-
-    @pl.when(~at_end)
-    def _():
-        start_p(1)
-        start_p(2)
+        zsteps(K3)
+        start_out(1)
+        start_out(2)
         steps_p((1, 2), True)
-        own_z(KB)
-
-    own_y(KB)
-
-    @pl.when(~at_end)
-    def _():
-        zsteps(KB)
-
+        own_out(KB)
+        own_y(KB)
+        steps_b()
+
+    wait_across(1)
+    hidden(1)
+    end_steps(1, 2)
     wait_across(last)
     steps_p((0,), False)
     hidden(last)
-    reduce(0, ffn_pair)
+    reduce(0, ffn_pair, (lambda: end_steps(2, Z - 1), lambda: end_steps(Z - 1, Z)))
     norm_to(res.at[0], update(0, xt, 1, 0.5), 2)
     wait_across(K3)
     steps_p((1, 2), False)
     unpack_edges()
     mixer()
-    reduce(1, mixer_pair)
+    reduce(1, mixer_pair, None)
     norm_to(res.at[1], update(1, res.at[0], 3, 1.0), 4)
 
     def again(k, carry):
@@ -916,7 +1004,7 @@
         return carry
 
     lax.fori_loop(0, nff, again, 0)
-    reduce(2, ffn_pair)
+    reduce(2, ffn_pair, None)
     update(2, res.at[1], 5, 0.5)
     outs = [
         pltpu.make_async_copy(
@@ -943,22 +1031,26 @@
             across(k, s, done)
             return carry
 
-        lax.fori_loop(0, Z, drain, 0)
+        lax.fori_loop(*((0, Z) if k < KB else (1, Z - 1)), drain, 0)
+    for q in range(4):
+        def drain_p(s, carry):
+            @pl.when((s <= z) & ((q < 3) | ~inside(s)))
+            def _():
+                right_p(q, s, done)
+
+            @pl.when((s >= z) & ((q < 3) | ~inside(s)))
+            def _():
+                left_p(q, s, done)
+
+            return carry
+
+        lax.fori_loop(0, Z, drain_p, 0)
     for q in range(3):
         across_p(q, f).wait_send()
 
-        def drain_p(s, carry):
-            @pl.when(s <= z)
-            def _():
-                right_p(q, s, done)
-
-            @pl.when(s >= z)
-            def _():
-                left_p(q, s, done)
-
-            return carry
-
-        lax.fori_loop(0, Z, drain_p, 0)
+    @pl.when(at_end)
+    def _():
+        across_p(3, f).wait_send()
 
     for r in range(3):
         def drain_r(s, carry):
@@ -1018,10 +1110,10 @@
                 dma((3 * nff + 8 + n_fs,)),
                 dma((nff + 2, 3, n_fs)),
                 dma((nff + 2, n_fs)),
-                dma((3, 2, Z)),
-                dma((3, Z)),
-                dma((3,)),
-                dma((3,)),
+                dma((4, 2, Z)),
+                dma((4, Z)),
+                dma((4,)),
+                dma((4,)),
                 dma((2, 3, Z)),
                 dma((2, 3, Z)),
                 dma((2, 3, Z)),

time: 187 us -> 183 us (0.979)
  Pallas kernels: 183 us -> 180 us
    pallas_call x1, Pallas kernels: 183 us -> 180 us  [local(): pl.pallas_call(functools.partial(stream_kernel, (Z, shard, part, width, h...]
where the time goes in v2:
time: 183 us; the launch traced here: 182 us
  Pallas kernels  180 us (98%)
  local copies, waits for them, and re-layouts  2.29 us (1%)
    pallas_call x1, Pallas kernels, local(): pl.pallas_call(functools.partial(stream_kernel, (Z, shard, part, width, h...  180 us

profile of v2, /device:TPU:0, one launch (start us, length us, event | category | flops | bytes accessed | tf_op | source)
XLA Modules:
  0.0 182.5 jit_solution(15875349560767242613)
XLA Ops:
  0.0 180.2 %shard_map.100 = bf16[2112,256]{1,0:T(8,128)(2,1)} custom-call(bf16[264,768]{1,0:T(8,128)(2,1)} %refs_0_.1, bf16[264,768]{1,0:T(8,128)(2,1)} %refs_1_.1, bf16[264,768]{1,0:T(8,128)(2,1)} %refs_2_.1, bf16[264,264]{1,0:T(8,128)(2,1)} %refs_3_.1, bf16[264,264]{1,0:T(8,128)(2,1)} %refs_4_.1, bf16[264,264]{1,0:T(8,128)(2,1)} %refs_5_.1, ...), custom_call_target="tpu_custom_call" | custom-call | tf_op jit(solution)/shard_map/pallas_call | solution.py:1083
  180.2 2.3 %copy.12 = bf16[256,2112]{0,1:T(8,128)(2,1)} copy(bf16[256,2112]{0,1:T(8,128)(2,1)} %bitcast.2) | data formatting | bytes 2162688

commit v3 on v2

--- a/solution.py
+++ b/solution.py
@@ -399,20 +399,22 @@
     own_refs = refs[:7]
     stream_ref, gains_ref, taps_ref, out_ref = refs[7:11]
     (ff, g3, gv, gb, pr, edge, xt, gtmp, gcol, gains, tbuf, normed, hid, mixed,
-     part_buf, crecv, xsend, xrecv, tot, res,
-     lsem, zsend, recv, psend, precv, pysend, pyrecv, csem, xsem, tsem, osem) = refs[11:]
+     part_buf, crecv, xsend, xrecv, tot, res, fd, acc,
+     lsem, zsend, recv, psend, precv, pysend, pyrecv, csem, xsem, tsem, osem,
+     dsem, hsem) = refs[11:]
     Y = 2
     n_fs = Z * Y
     rows = normed.shape[0]
     Dp = n_fs * shard
     groups = 128 // 32
     pair = Y * shard
-    last, K3, KB = nff - 1, nff, nff + 1
+    last, K3, KB = nff - 1, nff + 1, nff + 2
     f, t = lax.axis_index("fs"), lax.axis_index("tp")
     z, y = f // Y, f % Y
     c, x = t % 2, t // 2
     core_peer = (f, x * 2 + 1 - c)
     x_peer = (f, (1 - x) * 2 + c)
+    x_other = (f, (1 - x) * 2 + 1 - c)
     dev_y = (z * Y + (1 - y), t)
 
     def dev_z(zz):
@@ -424,16 +426,18 @@
     gate, up, down, ow, iw, vw, mw = own_refs
     moves = []
     for k in range(nff):
-        for j, w in enumerate((gate, up, down)):
-            moves.append((k, w.at[:, pl.ds(k * hc, hc)], ff.at[k, here, pl.ds(j * hc, hc)]))
+        moves.append((0, down.at[:, pl.ds(k * hc, hc)], ff.at[k, here, pl.ds(2 * hc, hc)]))
+    for k in range(nff):
+        for j, w in enumerate((gate, up)):
+            moves.append((k + 1, w.at[:, pl.ds(k * hc, hc)], ff.at[k, here, pl.ds(j * hc, hc)]))
     moves.append((K3, ow.at[:, lead], g3.at[here, lead]))
     moves.append((K3, iw.at[:, lead], g3.at[here, pl.ds(main, main)]))
     moves.append((K3, vw.at[:, lead], gv.at[here, lead]))
     moves.append((K3, mw.at[:, lead], gb.at[here, :]))
     for j, w in enumerate((ow, iw, vw, mw)):
-        moves.append((nff + 1, w, edge.at[j]))
+        moves.append((K3 + 1, w, edge.at[j]))
     for s in range(n_fs):
-        moves.append((nff + 2, stream_ref.at[pl.ds(s * part, part)], xt.at[pl.ds(s * shard, part)]))
+        moves.append((K3 + 2, stream_ref.at[pl.ds(s * part, part)], xt.at[pl.ds(s * shard, part)]))
     local = [
         (k, pltpu.make_async_copy(src, dst, lsem.at[n])) for n, (k, src, dst) in enumerate(moves)
     ]
@@ -447,6 +451,11 @@
             gv[pad] = jnp.zeros((shard - part, main + 128), BF16)
             gb[pad] = jnp.zeros((shard - part, main), BF16)
             xt[pad] = jnp.zeros((shard - part, rows), BF16)
+        for s in range(Z):
+            pad = pl.ds(s * shard + part, shard - part)
+            for i in range(1, 4):
+                for k in range(nff):
+                    fd[i, k, pad] = jnp.zeros((shard - part, hc), BF16)
 
     for _, copy in local:
         copy.start()
@@ -456,7 +465,7 @@
     def greet(d):
         pl.semaphore_signal(barrier, inc=1, device_id=d, device_id_type=MESH)
 
-    for d in (core_peer, x_peer, dev_y):
+    for d in (core_peer, x_peer, x_other, dev_y):
         greet(d)
 
     @pl.when(z > 0)
@@ -467,7 +476,7 @@
     def _():
         greet(dev_z(z + 1))
 
-    peers = 3 + (z > 0).astype(jnp.int32) + (z < Z - 1).astype(jnp.int32)
+    peers = 4 + (z > 0).astype(jnp.int32) + (z < Z - 1).astype(jnp.int32)
     pl.semaphore_wait(barrier, peers)
 
     def local_wait(k):
@@ -477,10 +486,12 @@
 
     def remote(k, s, way, d):
         at = pl.ds(pl.multiple_of(s * shard, 16), part)
-        if k < last:
-            ref = ff.at[k, at]
-        elif k == last:
-            ref = ff.at[k, at, 0 : 2 * hc]
+        if k == 0:
+            ref = ff.at[:, at, 2 * hc : 3 * hc]
+        elif k <= last:
+            ref = ff.at[k - 1, at, 0 : 2 * hc]
+        elif k == nff:
+            ref = ff.at[last, at, hc : 2 * hc]
         else:
             ref = (g3 if k == K3 else gb).at[at]
         return pltpu.make_async_remote_copy(
@@ -526,6 +537,25 @@
     def own_y(k):
         across(k, z, go)
 
+    def down_copy(kind, s, v):
+        to = (core_peer, x_peer, x_other)[kind]
+        return pltpu.make_async_remote_copy(
+            src_ref=ff.at[:, pl.ds(pl.multiple_of((s * Y + v) * shard, 16), part), 2 * hc : 3 * hc],
+            dst_ref=fd.at[kind + 1, :, pl.ds(pl.multiple_of(s * shard, 16), part)],
+            send_sem=dsem.at[0, kind, s], recv_sem=dsem.at[1, kind, s],
+            device_id=to, device_id_type=MESH,
+        )
+
+    def spread(s, v, act):
+        @pl.when(v == c)
+        def _():
+            act(down_copy(1, s, v))
+
+        @pl.when(v != c)
+        def _():
+            act(down_copy(2, s, v))
+            act(down_copy(0, s, v))
+
     def zsteps(k):
         def step(i, carry):
             @pl.when(z - 1 - i >= 0)
@@ -534,6 +564,8 @@
                 remote(k, s * Y + y, 0, dev_z(z - 1)).wait_recv()
                 right(k, s, go)
                 across(k, s, go)
+                if k == 0:
+                    spread(s, y, go)
 
             @pl.when(z + 1 + i < Z)
             def _():
@@ -541,6 +573,8 @@
                 remote(k, s * Y + y, 0, dev_z(z + 1)).wait_recv()
                 left(k, s, go)
                 across(k, s, go)
+                if k == 0:
+                    spread(s, y, go)
 
             return carry
 
@@ -559,7 +593,7 @@
         at = pl.ds(pl.multiple_of(first * shard, 16), (count - 1) * shard + part)
         if q == 3:
             return gb.at[at]
-        return gv.at[at, lead] if q == 1 else ff.at[last, at, 2 * hc : 3 * hc]
+        return gv.at[at, lead] if q == 1 else ff.at[last, at, 0:hc]
 
     def across_p(q, s):
         ref = piece(q, s, 1)
@@ -766,23 +800,90 @@
 
         return lax.fori_loop(0, nblk, body, jnp.zeros((8, rows), F32))
 
-    def hidden(k):
+    def hidden_copy(u, kind, k):
+        source = hid.at[u, 2 if kind == 2 else 0, k]
+        return pltpu.make_async_remote_copy(
+            src_ref=source, dst_ref=hid.at[u, kind + 1, k], send_sem=hsem.at[0, u, kind, k],
+            recv_sem=hsem.at[1, u, kind, k], device_id=x_peer if kind == 1 else core_peer,
+            device_id_type=MESH,
+        )
+
+    def hidden(u, k):
         n = normed[...]
         gate_v = jnp.dot(n, ff[k, :, 0:hc], preferred_element_type=F32)
         up_v = jnp.dot(n, ff[k, :, hc : 2 * hc], preferred_element_type=F32)
-        hid[k] = (gate_v / (1.0 + jnp.exp(-gate_v)) * up_v).astype(BF16)
+        hid[u, 0, k] = (gate_v / (1.0 + jnp.exp(-gate_v)) * up_v).astype(BF16)
+        hidden_copy(u, 1, k).start()
+        hidden_copy(u, 0, k).start()
+
+    def product(u, i, k, at):
+        return lax.dot_general(fd[i, k, at], hid[u, i, k], NT, preferred_element_type=F32)
+
+    def keep_down():
+        def body(s, carry):
+            at = pl.ds(pl.multiple_of(s * shard, 16), shard)
+            for k in range(nff):
+                fd[0, k, at] = ff[
+                    k, pl.ds(pl.multiple_of((s * Y + c) * shard, 16), shard), 2 * hc : 3 * hc
+                ]
+            return carry
+
+        lax.fori_loop(0, Z, body, 0)
+
+    def finish_ffn(u, r, hook):
+        def rows_of(j):
+            return pl.ds(pl.multiple_of(j * shard, 16), shard)
+
+        def own_part(j, carry):
+            at = rows_of(j)
+            total = product(u, 0, 0, at)
+            for k in range(1, nff):
+                total = total + product(u, 0, k, at)
+            acc[at] = total
+            return carry
+
+        def add(i, ks):
+            def body(j, carry):
+                at = rows_of(j)
+                total = acc[at]
+                for k in ks:
+                    total = total + product(u, i, k, at)
+                acc[at] = total
+                return carry
+
+            lax.fori_loop(0, Z, body, 0)
+
+        lax.fori_loop(0, Z, own_part, 0)
+        for k in range(nff):
+            hidden_copy(u, 0, k).wait_recv()
+        add(1, range(nff))
+        for k in range(nff):
+            hidden_copy(u, 1, k).wait_recv()
+            hidden_copy(u, 2, k).start()
+            if k > 0:
+                hidden_copy(u, 2, k - 1).wait_recv()
+                add(3, (k - 1,))
+            add(2, (k,))
+        if hook:
+            hook()
+        hidden_copy(u, 2, last).wait_recv()
+
+        def final(j, carry):
+            at = rows_of(j)
+            to = pl.ds(pl.multiple_of(j * pair + c * shard, 16), shard)
+            tot[r, to] = (acc[at] + product(u, 3, last, at)).astype(BF16)
+            tot_copy(r, j).start()
+            return carry
+
+        def arrive(j, carry):
+            tot_copy(r, j).wait_recv()
+            return carry
+
+        lax.fori_loop(0, Z, final, 0)
+        lax.fori_loop(0, Z, arrive, 0)
 
     def pair_at(j):
         return pl.ds(pl.multiple_of(j * pair, 16), pair)
-
-    def ffn_pair(r, j):
-        at = pair_at(j)
-        total = lax.dot_general(ff[0, at, 2 * hc :], hid[0], NT, preferred_element_type=F32)
-        for k in range(1, nff):
-            total = total + lax.dot_general(
-                ff[k, at, 2 * hc :], hid[k], NT, preferred_element_type=F32
-            )
-        part_buf[r, j] = total.astype(BF16)
 
     def mixer_pair(r, j):
         @pl.when(inside(j))
@@ -794,21 +895,21 @@
         total = total + lax.dot_general(
             gv[at, main : main + 128], mixed[:, main:], NT, preferred_element_type=F32
         )
-        part_buf[r, j] = total.astype(BF16)
+        part_buf[j] = total.astype(BF16)
 
     mine = pl.ds(pl.multiple_of(c * shard, 16), shard)
     other = pl.ds(pl.multiple_of((1 - c) * shard, 16), shard)
 
     def core_copy(r, j):
         return pltpu.make_async_remote_copy(
-            src_ref=part_buf.at[r, j, other], dst_ref=crecv.at[r, j], send_sem=csem.at[0, r, j],
-            recv_sem=csem.at[1, r, j], device_id=core_peer, device_id_type=MESH,
+            src_ref=part_buf.at[j, other], dst_ref=crecv.at[j], send_sem=csem.at[0, j],
+            recv_sem=csem.at[1, j], device_id=core_peer, device_id_type=MESH,
         )
 
     def x_copy(r, j):
         return pltpu.make_async_remote_copy(
-            src_ref=xsend.at[r, j], dst_ref=xrecv.at[r, j], send_sem=xsem.at[0, r, j],
-            recv_sem=xsem.at[1, r, j], device_id=x_peer, device_id_type=MESH,
+            src_ref=xsend.at[j], dst_ref=xrecv.at[j], send_sem=xsem.at[0, j],
+            recv_sem=xsem.at[1, j], device_id=x_peer, device_id_type=MESH,
         )
 
     def tot_copy(r, j):
@@ -848,20 +949,17 @@
         def _():
             lax.fori_loop(first, stop, step, 0)
 
-    def reduce(r, compute, hooks):
+    def reduce(r, compute):
         def cross(j):
             core_copy(r, j).wait_recv()
-            xsend[r, j] = (
-                part_buf[r, j, mine].astype(F32) + crecv[r, j].astype(F32)
-            ).astype(BF16)
+            xsend[j] = (part_buf[j, mine].astype(F32) + crecv[j].astype(F32)).astype(BF16)
             x_copy(r, j).start()
 
         def send(s, carry):
             j = order(s)
-            if r == 1:
-                @pl.when(at_end & (s < Z - 1))
-                def _():
-                    pass_on(order(s + 1))
+            @pl.when(at_end & (s < Z - 1))
+            def _():
+                pass_on(order(s + 1))
 
             compute(r, j)
             core_copy(r, j).start()
@@ -876,7 +974,7 @@
             j = order(s)
             x_copy(r, j).wait_recv()
             at = pl.ds(pl.multiple_of(j * pair + c * shard, 16), shard)
-            tot[r, at] = (xsend[r, j].astype(F32) + xrecv[r, j].astype(F32)).astype(BF16)
+            tot[r, at] = (xsend[j].astype(F32) + xrecv[j].astype(F32)).astype(BF16)
             tot_copy(r, j).start()
             return carry
 
@@ -886,12 +984,7 @@
 
         lax.fori_loop(0, Z, send, 0)
         cross(order(Z - 1))
-        if hooks:
-            hooks[0]()
-        lax.fori_loop(0, Z // 2, receive, 0)
-        if hooks:
-            hooks[1]()
-        lax.fori_loop(Z // 2, Z, receive, 0)
+        lax.fori_loop(0, Z, receive, 0)
         lax.fori_loop(0, Z, finish, 0)
 
     def mixer():
@@ -921,17 +1014,26 @@
                 conv = conv + tbuf[j : j + 1, first : first + lanes] * moved
             mixed[:, first : first + lanes] = (outer * conv).astype(BF16)
 
+    def spread_across(s, carry):
+        j = order(s)
+        remote(0, j * Y + 1 - y, 2, dev_y).wait_recv()
+        spread(j, 1 - y, go)
+        return carry
+
     for k in range(2):
         local_wait(k)
         own_in(k)
         own_out(k)
         own_y(k)
-    local_wait(nff + 1)
+        if k == 0:
+            spread(z, y, go)
+    local_wait(K3 + 1)
     pack_edges()
-    for k in range(2, nff + 1):
+    for k in range(2, K3 + 1):
         local_wait(k)
     for q in range(3):
         across_p(q, f).start()
+
     @pl.when(at_end)
     def _():
         across_p(3, f).start()
@@ -940,11 +1042,13 @@
 
     own_out(2)
     own_y(2)
-    local_wait(nff + 2)
+    local_wait(K3 + 2)
     prepare_gains()
     prepare_taps()
     norm_to(xt, sum_squares(xt), 0)
     zsteps(0)
+    own_out(nff)
+    own_y(nff)
 
     @pl.when(~at_end)
     def _():
@@ -959,6 +1063,13 @@
             start_in(q)
 
     zsteps(1)
+    lax.fori_loop(0, Z // 2, spread_across, 0)
+
+    @pl.when(~at_end)
+    def _():
+        own_in(nff)
+
+    zsteps(2)
     own_out(K3)
 
     @pl.when(~at_end)
@@ -968,11 +1079,13 @@
         start_in(2)
         own_in(KB)
 
-    wait_across(0)
-    hidden(0)
-    zsteps(last)
+    lax.fori_loop(Z // 2, Z, spread_across, 0)
+    zsteps(nff)
     steps_p((0,), True)
     own_y(K3)
+    keep_down()
+    wait_across(1)
+    hidden(0, 0)
 
     @pl.when(~at_end)
     def _():
@@ -984,27 +1097,35 @@
         own_y(KB)
         steps_b()
 
-    wait_across(1)
-    hidden(1)
+    wait_across(2)
+    hidden(0, 1)
+
+    def down_arrived(s, carry):
+        for kind in range(3):
+            down_copy(kind, s, c).wait_recv()
+        return carry
+
     end_steps(1, 2)
-    wait_across(last)
+    lax.fori_loop(0, Z, down_arrived, 0)
+    wait_across(nff)
     steps_p((0,), False)
-    hidden(last)
-    reduce(0, ffn_pair, (lambda: end_steps(2, Z - 1), lambda: end_steps(Z - 1, Z)))
+    hidden(0, last)
+    finish_ffn(0, 0, lambda: end_steps(2, Z - 1))
     norm_to(res.at[0], update(0, xt, 1, 0.5), 2)
+    end_steps(Z - 1, Z)
     wait_across(K3)
     steps_p((1, 2), False)
     unpack_edges()
     mixer()
-    reduce(1, mixer_pair, None)
+    reduce(1, mixer_pair)
     norm_to(res.at[1], update(1, res.at[0], 3, 1.0), 4)
 
     def again(k, carry):
-        hidden(k)
+        hidden(1, k)
         return carry
 
     lax.fori_loop(0, nff, again, 0)
-    reduce(2, ffn_pair, None)
+    finish_ffn(1, 2, None)
     update(2, res.at[1], 5, 0.5)
     outs = [
         pltpu.make_async_copy(
@@ -1018,7 +1139,7 @@
     def done(copy):
         copy.wait_send()
 
-    for k in range(nff + 2):
+    for k in range(nff + 3):
         def drain(s, carry):
             @pl.when(s <= z)
             def _():
@@ -1052,14 +1173,20 @@
     def _():
         across_p(3, f).wait_send()
 
-    for r in range(3):
-        def drain_r(s, carry):
-            core_copy(r, s).wait_send()
-            x_copy(r, s).wait_send()
+    def drain_r(s, carry):
+        core_copy(1, s).wait_send()
+        x_copy(1, s).wait_send()
+        for r in range(3):
             tot_copy(r, s).wait_send()
-            return carry
-
-        lax.fori_loop(0, Z, drain_r, 0)
+        for v in range(Y):
+            spread(s, v, done)
+        return carry
+
+    lax.fori_loop(0, Z, drain_r, 0)
+    for u in range(2):
+        for kind in range(3):
+            for k in range(nff):
+                hidden_copy(u, kind, k).wait_send()
     for copy in outs:
         copy.wait()
 
@@ -1099,25 +1226,29 @@
                 vmem((6, Dp, 128), F32),
                 vmem((8, taps), F32),
                 vmem((rows, Dp), BF16),
-                vmem((nff, rows, hc), BF16),
+                vmem((2, 4, nff, rows, hc), BF16),
                 vmem((rows, main + 128), BF16),
-                vmem((3, Z, 2 * shard, rows), BF16),
-                vmem((3, Z, shard, rows), BF16),
-                vmem((3, Z, shard, rows), BF16),
-                vmem((3, Z, shard, rows), BF16),
+                vmem((Z, 2 * shard, rows), BF16),
+                vmem((Z, shard, rows), BF16),
+                vmem((Z, shard, rows), BF16),
+                vmem((Z, shard, rows), BF16),
                 vmem((3, Dp, rows), BF16),
                 vmem((3, Dp, rows), BF16),
+                vmem((4, nff, Z * shard, hc), BF16),
+                vmem((Z * shard, rows), F32),
                 dma((3 * nff + 8 + n_fs,)),
-                dma((nff + 2, 3, n_fs)),
-                dma((nff + 2, n_fs)),
+                dma((nff + 3, 3, n_fs)),
+                dma((nff + 3, n_fs)),
                 dma((4, 2, Z)),
                 dma((4, Z)),
                 dma((4,)),
                 dma((4,)),
-                dma((2, 3, Z)),
-                dma((2, 3, Z)),
+                dma((2, Z)),
+                dma((2, Z)),
                 dma((2, 3, Z)),
                 dma((n_fs,)),
+                dma((2, 3, Z)),
+                dma((2, 2, 3, nff)),
             ],
             compiler_params=pltpu.CompilerParams(
                 collective_id=0, has_side_effects=True, vmem_limit_bytes=60 * 1024 * 1024

time: 183 us -> 179 us (0.978)
  Pallas kernels: 180 us -> 177 us
    pallas_call x1, Pallas kernels: 180 us -> 177 us  [local(): pl.pallas_call(functools.partial(stream_kernel, (Z, shard, part, width, h...]
where the time goes in v3:
time: 179 us
  Pallas kernels  177 us (99%)
  local copies, waits for them, and re-layouts  2.29 us (1%)
    pallas_call x1, Pallas kernels, local(): pl.pallas_call(functools.partial(stream_kernel, (Z, shard, part, width, h...  177 us

profile of v3, /device:TPU:0, one launch (start us, length us, event | category | flops | bytes accessed | tf_op | source)
XLA Modules:
  0.0 179.2 jit_solution(15221774704445045524)
XLA Ops:
  0.0 177.0 %shard_map.100 = bf16[2112,256]{1,0:T(8,128)(2,1)} custom-call(bf16[264,768]{1,0:T(8,128)(2,1)} %refs_0_.1, bf16[264,768]{1,0:T(8,128)(2,1)} %refs_1_.1, bf16[264,768]{1,0:T(8,128)(2,1)} %refs_2_.1, bf16[264,264]{1,0:T(8,128)(2,1)} %refs_3_.1, bf16[264,264]{1,0:T(8,128)(2,1)} %refs_4_.1, bf16[264,264]{1,0:T(8,128)(2,1)} %refs_5_.1, ...), custom_call_target="tpu_custom_call" | custom-call | tf_op jit(solution)/shard_map/pallas_call | solution.py:1210
  177.0 2.3 %copy.12 = bf16[256,2112]{0,1:T(8,128)(2,1)} copy(bf16[256,2112]{0,1:T(8,128)(2,1)} %bitcast.2) | data formatting | bytes 2162688

commit v4 on v3

--- a/solution.py
+++ b/solution.py
@@ -398,9 +398,9 @@
     Z, shard, part, width, hc, nff, main, rem, grp = cfg
     own_refs = refs[:7]
     stream_ref, gains_ref, taps_ref, out_ref = refs[7:11]
-    (ff, g3, gv, gb, pr, edge, xt, gtmp, gcol, gains, tbuf, normed, hid, mixed,
+    (ff, g3, gv, gb, pr, edge, xt, gains_in, taps_in, gtmp, gcol, gains, tbuf, normed, hid, mixed,
      part_buf, crecv, xsend, xrecv, tot, res, fd, acc,
-     lsem, zsend, recv, psend, precv, pysend, pyrecv, csem, xsem, tsem, osem,
+     lsem, zsend, recv, psend, precv, pysend, pyrecv, csem, xsem, tsem,
      dsem, hsem) = refs[11:]
     Y = 2
     n_fs = Z * Y
@@ -436,30 +436,42 @@
     moves.append((K3, mw.at[:, lead], gb.at[here, :]))
     for j, w in enumerate((ow, iw, vw, mw)):
         moves.append((K3 + 1, w, edge.at[j]))
+    moves.append((K3 + 2, gains_ref, gains_in))
+    moves.append((K3 + 2, taps_ref, taps_in))
     for s in range(n_fs):
         moves.append((K3 + 2, stream_ref.at[pl.ds(s * part, part)], xt.at[pl.ds(s * shard, part)]))
     local = [
         (k, pltpu.make_async_copy(src, dst, lsem.at[n])) for n, (k, src, dst) in enumerate(moves)
     ]
 
-    def clear_pads():
-        for s in range(n_fs):
-            pad = pl.ds(s * shard + part, shard - part)
+    def pads(count):
+        return [pl.ds(s * shard + part, shard - part) for s in range(count)]
+
+    def clear(ref, index):
+        ref[index] = jnp.zeros(ref.at[index].shape, ref.dtype)
+
+    def clear_pairs():
+        for pad in pads(n_fs):
+            clear(ff, (last, pad, pl.ds(0, hc)))
+            clear(gv, (pad, lead))
+            clear(gb, (pad,))
+
+    def clear_rest():
+        for pad in pads(n_fs):
             for k in range(nff):
-                ff[k, pad] = jnp.zeros((shard - part, 3 * hc), BF16)
-            g3[pad] = jnp.zeros((shard - part, 2 * main), BF16)
-            gv[pad] = jnp.zeros((shard - part, main + 128), BF16)
-            gb[pad] = jnp.zeros((shard - part, main), BF16)
-            xt[pad] = jnp.zeros((shard - part, rows), BF16)
-        for s in range(Z):
-            pad = pl.ds(s * shard + part, shard - part)
+                clear(ff, (k, pad, pl.ds(0 if k < last else hc, 3 * hc if k < last else 2 * hc)))
+            clear(g3, (pad,))
+            clear(gv, (pad, pl.ds(main, 128)))
+            clear(xt, (pad,))
+        for pad in pads(Z):
             for i in range(1, 4):
                 for k in range(nff):
-                    fd[i, k, pad] = jnp.zeros((shard - part, hc), BF16)
-
-    for _, copy in local:
-        copy.start()
-    clear_pads()
+                    clear(fd, (i, k, pad))
+
+    for owner, copy in local:
+        if owner < 2:
+            copy.start()
+    clear_pairs()
     barrier = pltpu.get_barrier_semaphore()
 
     def greet(d):
@@ -476,6 +488,10 @@
     def _():
         greet(dev_z(z + 1))
 
+    for owner, copy in local:
+        if owner >= 2:
+            copy.start()
+    clear_rest()
     peers = 4 + (z > 0).astype(jnp.int32) + (z < Z - 1).astype(jnp.int32)
     pl.semaphore_wait(barrier, peers)
 
@@ -709,7 +725,7 @@
         row = lax.broadcasted_iota(jnp.int32, (128, 128), 0)
         lane = lax.broadcasted_iota(jnp.int32, (128, 128), 1)
 
-        def body(s, carry):
+        def unpack(s):
             packed = pr[pl.ds(pl.multiple_of(s * grp, 16), grp)]
             for j in range(groups):
                 count = min(grp, shard - j * grp)
@@ -719,13 +735,23 @@
                 block = jnp.dot(packed, pick, preferred_element_type=F32)[:count]
                 at = pl.ds(pl.multiple_of(s * shard + j * grp, 16), count)
                 gv[at, main : main + 128] = block.astype(BF16)
-            return carry
-
-        lax.fori_loop(0, n_fs, body, 0)
+
+        def body(i, carry):
+            j = order(i)
+
+            @pl.when(at_end & (i > 0))
+            def _():
+                remote_p(2, j, 0, toward()).wait_recv()
+
+            for v in range(Y):
+                unpack(j * Y + v)
+            return carry
+
+        lax.fori_loop(0, Z, body, 0)
 
     def prepare_gains():
         gtmp[...] = jnp.zeros(gtmp.shape, F32)
-        gtmp[0:6, 0:width] = gains_ref[...]
+        gtmp[0:6, 0:width] = gains_in[...]
         for i in range(gtmp.shape[1] // 128):
             gcol[i * 128 : (i + 1) * 128] = gtmp[:, i * 128 : (i + 1) * 128].T
 
@@ -742,10 +768,10 @@
 
     def prepare_taps():
         n_tp = lax.axis_size("tp")
-        channels = taps_ref.shape[1] // n_tp
+        channels = taps_in.shape[1] // n_tp
         lanes = tbuf.shape[1]
         tbuf[...] = jnp.zeros(tbuf.shape, F32)
-        tbuf[0:CONV_K, 0 : taps_ref.shape[1]] = taps_ref[...].astype(F32)
+        tbuf[0:CONV_K, 0 : taps_in.shape[1]] = taps_in[...].astype(F32)
         full = tbuf[...]
         mine = full
         for i in range(1, n_tp):
@@ -759,7 +785,7 @@
     nblk = Dp // BLK
 
     def squares(v):
-        return jnp.sum((v * v).reshape(BLK // 8, 8, rows), axis=0)
+        return jnp.sum((v * v).reshape(v.shape[0] // 8, 8, rows), axis=0)
 
     def block_at(i):
         return pl.ds(pl.multiple_of(i * BLK, BLK), BLK)
@@ -788,8 +814,8 @@
 
         lax.fori_loop(0, nblk, body, 0)
 
-    def update(r, source, row, factor):
-        scale = inverse(sum_squares(tot.at[r])) * factor
+    def update(r, sums, source, row, factor):
+        scale = inverse(sums) * factor
 
         def body(i, sums):
             at = block_at(i)
@@ -830,7 +856,7 @@
 
         lax.fori_loop(0, Z, body, 0)
 
-    def finish_ffn(u, r, hook):
+    def finish_ffn(u, r, hook, idle):
         def rows_of(j):
             return pl.ds(pl.multiple_of(j * shard, 16), shard)
 
@@ -857,6 +883,8 @@
         for k in range(nff):
             hidden_copy(u, 0, k).wait_recv()
         add(1, range(nff))
+        if idle:
+            idle()
         for k in range(nff):
             hidden_copy(u, 1, k).wait_recv()
             hidden_copy(u, 2, k).start()
@@ -868,19 +896,14 @@
             hook()
         hidden_copy(u, 2, last).wait_recv()
 
-        def final(j, carry):
+        def final(j, sums):
             at = rows_of(j)
-            to = pl.ds(pl.multiple_of(j * pair + c * shard, 16), shard)
-            tot[r, to] = (acc[at] + product(u, 3, last, at)).astype(BF16)
+            v = (acc[at] + product(u, 3, last, at)).astype(BF16)
+            tot[r, column(j, c)] = v
             tot_copy(r, j).start()
-            return carry
-
-        def arrive(j, carry):
-            tot_copy(r, j).wait_recv()
-            return carry
-
-        lax.fori_loop(0, Z, final, 0)
-        lax.fori_loop(0, Z, arrive, 0)
+            return sums + squares(v.astype(F32))
+
+        return both_squares(r, lax.fori_loop(0, Z, final, jnp.zeros((8, rows), F32)), lambda j: j)
 
     def pair_at(j):
         return pl.ds(pl.multiple_of(j * pair, 16), pair)
@@ -912,12 +935,25 @@
             recv_sem=xsem.at[1, j], device_id=x_peer, device_id_type=MESH,
         )
 
+    def column(j, v):
+        return pl.ds(pl.multiple_of(j * pair + v * shard, 16), shard)
+
+    def both_squares(r, mine_sums, at):
+        def arrive(s, sums):
+            tot_copy(r, at(s)).wait_recv()
+            return sums + squares(tot[r, column(at(s), 1 - c)].astype(F32))
+
+        return mine_sums + lax.fori_loop(0, Z, arrive, jnp.zeros((8, rows), F32))
+
     def tot_copy(r, j):
-        at = pl.ds(pl.multiple_of(j * pair + c * shard, 16), shard)
+        at = column(j, c)
         return pltpu.make_async_remote_copy(
             src_ref=tot.at[r, at], dst_ref=tot.at[r, at], send_sem=tsem.at[0, r, j],
             recv_sem=tsem.at[1, r, j], device_id=core_peer, device_id_type=MESH,
         )
+
+    def toward():
+        return dev_z(jnp.where(z == 0, z + 1, z - 1))
 
     def order(s):
         step = (s + 1) // 2
@@ -925,7 +961,7 @@
         return jnp.where(s <= 2 * near, close, jnp.where(low, s, Z - 1 - s))
 
     def pass_on(j):
-        source = dev_z(jnp.where(z == 0, z + 1, z - 1))
+        source = toward()
 
         @pl.when(inside(j))
         def _():
@@ -937,7 +973,7 @@
             remote_p(3, j, 0, source).wait_recv()
 
     def end_steps(first, stop):
-        source = dev_z(jnp.where(z == 0, z + 1, z - 1))
+        source = toward()
 
         def step(s, carry):
             j = order(s)
@@ -957,7 +993,7 @@
 
         def send(s, carry):
             j = order(s)
-            @pl.when(at_end & (s < Z - 1))
+            @pl.when(at_end & (s > 0) & (s < Z - 1))
             def _():
                 pass_on(order(s + 1))
 
@@ -970,22 +1006,17 @@
 
             return carry
 
-        def receive(s, carry):
+        def receive(s, sums):
             j = order(s)
             x_copy(r, j).wait_recv()
-            at = pl.ds(pl.multiple_of(j * pair + c * shard, 16), shard)
-            tot[r, at] = (xsend[j].astype(F32) + xrecv[j].astype(F32)).astype(BF16)
+            v = (xsend[j].astype(F32) + xrecv[j].astype(F32)).astype(BF16)
+            tot[r, column(j, c)] = v
             tot_copy(r, j).start()
-            return carry
-
-        def finish(s, carry):
-            tot_copy(r, order(s)).wait_recv()
-            return carry
+            return sums + squares(v.astype(F32))
 
         lax.fori_loop(0, Z, send, 0)
         cross(order(Z - 1))
-        lax.fori_loop(0, Z, receive, 0)
-        lax.fori_loop(0, Z, finish, 0)
+        return both_squares(r, lax.fori_loop(0, Z, receive, jnp.zeros((8, rows), F32)), order)
 
     def mixer():
         n = normed[...]
@@ -993,6 +1024,11 @@
         outer_inner = outer_inner.astype(BF16).astype(F32)
         value_rest = jnp.dot(n, gv[...], preferred_element_type=F32)
         value_rest = value_rest.astype(BF16).astype(F32)
+
+        @pl.when(at_end)
+        def _():
+            pass_on(order(1))
+
         rest = value_rest[:, main:]
         lane = lax.broadcasted_iota(jnp.int32, rest.shape, 1)
         keep = (lane >= 3 * rem) & (lane < 4 * rem)
@@ -1014,6 +1050,58 @@
                 conv = conv + tbuf[j : j + 1, first : first + lanes] * moved
             mixed[:, first : first + lanes] = (outer * conv).astype(BF16)
 
+    def drain_all():
+        def done(copy):
+            copy.wait_send()
+
+        for k in range(nff + 3):
+            def drain(s, carry):
+                @pl.when(s <= z)
+                def _():
+                    right(k, s, done)
+
+                @pl.when(s >= z)
+                def _():
+                    left(k, s, done)
+
+                across(k, s, done)
+                return carry
+
+            lax.fori_loop(*((0, Z) if k < KB else (1, Z - 1)), drain, 0)
+        for q in range(4):
+            def drain_p(s, carry):
+                @pl.when((s <= z) & ((q < 3) | ~inside(s)))
+                def _():
+                    right_p(q, s, done)
+
+                @pl.when((s >= z) & ((q < 3) | ~inside(s)))
+                def _():
+                    left_p(q, s, done)
+
+                return carry
+
+            lax.fori_loop(0, Z, drain_p, 0)
+        for q in range(3):
+            across_p(q, f).wait_send()
+
+        @pl.when(at_end)
+        def _():
+            across_p(3, f).wait_send()
+
+        def drain_r(s, carry):
+            core_copy(1, s).wait_send()
+            x_copy(1, s).wait_send()
+            for r in range(2):
+                tot_copy(r, s).wait_send()
+            for v in range(Y):
+                spread(s, v, done)
+            return carry
+
+        lax.fori_loop(0, Z, drain_r, 0)
+        for kind in range(3):
+            for k in range(nff):
+                hidden_copy(0, kind, k).wait_send()
+
     def spread_across(s, carry):
         j = order(s)
         remote(0, j * Y + 1 - y, 2, dev_y).wait_recv()
@@ -1110,85 +1198,34 @@
     wait_across(nff)
     steps_p((0,), False)
     hidden(0, last)
-    finish_ffn(0, 0, lambda: end_steps(2, Z - 1))
-    norm_to(res.at[0], update(0, xt, 1, 0.5), 2)
+    sums = finish_ffn(0, 0, lambda: end_steps(2, Z - 1), None)
+    norm_to(res.at[0], update(0, sums, xt, 1, 0.5), 2)
     end_steps(Z - 1, Z)
     wait_across(K3)
-    steps_p((1, 2), False)
     unpack_edges()
+    steps_p((1,), False)
     mixer()
-    reduce(1, mixer_pair)
-    norm_to(res.at[1], update(1, res.at[0], 3, 1.0), 4)
+    sums = reduce(1, mixer_pair)
+    norm_to(res.at[1], update(1, sums, res.at[0], 3, 1.0), 4)
 
     def again(k, carry):
         hidden(1, k)
         return carry
 
     lax.fori_loop(0, nff, again, 0)
-    finish_ffn(1, 2, None)
-    update(2, res.at[1], 5, 0.5)
-    outs = [
-        pltpu.make_async_copy(
-            res.at[2, pl.ds(s * shard, part)], out_ref.at[pl.ds(s * part, part)], osem.at[s]
-        )
-        for s in range(n_fs)
-    ]
-    for copy in outs:
-        copy.start()
-
-    def done(copy):
-        copy.wait_send()
-
-    for k in range(nff + 3):
-        def drain(s, carry):
-            @pl.when(s <= z)
-            def _():
-                right(k, s, done)
-
-            @pl.when(s >= z)
-            def _():
-                left(k, s, done)
-
-            across(k, s, done)
-            return carry
-
-        lax.fori_loop(*((0, Z) if k < KB else (1, Z - 1)), drain, 0)
-    for q in range(4):
-        def drain_p(s, carry):
-            @pl.when((s <= z) & ((q < 3) | ~inside(s)))
-            def _():
-                right_p(q, s, done)
-
-            @pl.when((s >= z) & ((q < 3) | ~inside(s)))
-            def _():
-                left_p(q, s, done)
-
-            return carry
-
-        lax.fori_loop(0, Z, drain_p, 0)
-    for q in range(3):
-        across_p(q, f).wait_send()
-
-    @pl.when(at_end)
-    def _():
-        across_p(3, f).wait_send()
-
-    def drain_r(s, carry):
-        core_copy(1, s).wait_send()
-        x_copy(1, s).wait_send()
-        for r in range(3):
-            tot_copy(r, s).wait_send()
-        for v in range(Y):
-            spread(s, v, done)
+    scale = inverse(finish_ffn(1, 2, None, drain_all)) * 0.5
+    for s in range(n_fs):
+        at = pl.ds(s * shard, part)
+        v = res[1, at].astype(F32) + tot[2, at].astype(F32) * scale * gain_block(5, at)
+        out_ref[s * part : (s + 1) * part] = v.astype(BF16)
+    def drain_last(j, carry):
+        tot_copy(2, j).wait_send()
         return carry
 
-    lax.fori_loop(0, Z, drain_r, 0)
-    for u in range(2):
-        for kind in range(3):
-            for k in range(nff):
-                hidden_copy(u, kind, k).wait_send()
-    for copy in outs:
-        copy.wait()
+    lax.fori_loop(0, Z, drain_last, 0)
+    for kind in range(3):
+        for k in range(nff):
+            hidden_copy(1, kind, k).wait_send()
 
 
 def stream_form(mesh, Z):
@@ -1209,10 +1246,9 @@
         dma, vmem = pltpu.SemaphoreType.DMA, pltpu.VMEM
         out = pl.pallas_call(
             functools.partial(stream_kernel, (Z, shard, part, width, hc, nff, main, rem, grp)),
-            out_shape=jax.ShapeDtypeStruct((width, rows), BF16),
-            in_specs=[pl.BlockSpec(memory_space=pl.ANY)] * 8
-            + [pl.BlockSpec(memory_space=pltpu.VMEM)] * 2,
-            out_specs=pl.BlockSpec(memory_space=pl.ANY),
+            out_shape=pltpu.VMEM((width, rows), BF16),
+            in_specs=[pl.BlockSpec(memory_space=pl.ANY)] * 10,
+            out_specs=pl.BlockSpec(memory_space=pltpu.VMEM),
             scratch_shapes=[
                 vmem((nff, Dp, 3 * hc), BF16),
                 vmem((Dp, 2 * main), BF16),
@@ -1221,6 +1257,8 @@
                 vmem((n_fs * grp, 128), BF16),
                 vmem((4, part, channels), BF16),
                 vmem((Dp, rows), BF16),
+                vmem(norm_gains.shape, F32),
+                vmem(conv_taps.shape, BF16),
                 vmem((128, lanes), F32),
                 vmem((lanes, 128), F32),
                 vmem((6, Dp, 128), F32),
@@ -1233,10 +1271,10 @@
                 vmem((Z, shard, rows), BF16),
                 vmem((Z, shard, rows), BF16),
                 vmem((3, Dp, rows), BF16),
-                vmem((3, Dp, rows), BF16),
+                vmem((2, Dp, rows), BF16),
                 vmem((4, nff, Z * shard, hc), BF16),
                 vmem((Z * shard, rows), F32),
-                dma((3 * nff + 8 + n_fs,)),
+                dma((3 * nff + 10 + n_fs,)),
                 dma((nff + 3, 3, n_fs)),
                 dma((nff + 3, n_fs)),
                 dma((4, 2, Z)),
@@ -1246,7 +1284,6 @@
                 dma((2, Z)),
                 dma((2, Z)),
                 dma((2, 3, Z)),
-                dma((n_fs,)),
                 dma((2, 3, Z)),
                 dma((2, 2, 3, nff)),
             ],

time: 179 us -> 176 us (0.983)
  Pallas kernels: 177 us -> 175 us
    pallas_call x1, Pallas kernels: 177 us -> 175 us  [local(): pl.pallas_call(functools.partial(stream_kernel, (Z, shard, part, width, h...]
where the time goes in v4:
time: 176 us
  Pallas kernels  175 us (99%)
    pallas_call x1, Pallas kernels, local(): pl.pallas_call(functools.partial(stream_kernel, (Z, shard, part, width, h...  175 us

profile of v4, /device:TPU:0, one launch (start us, length us, event | category | flops | bytes accessed | tf_op | source)
XLA Modules:
  0.0 175.6 jit_solution(3160280222528016321)
XLA Ops:
  0.0 174.6 %shard_map.100 = bf16[2112,256]{1,0:T(8,128)(2,1)S(1)} custom-call(bf16[264,768]{1,0:T(8,128)(2,1)} %refs_0_.1, bf16[264,768]{1,0:T(8,128)(2,1)} %refs_1_.1, bf16[264,768]{1,0:T(8,128)(2,1)} %refs_2_.1, bf16[264,264]{1,0:T(8,128)(2,1)} %refs_3_.1, bf16[264,264]{1,0:T(8,128)(2,1)} %refs_4_.1, bf16[264,264]{1,0:T(8,128)(2,1)} %refs_5_.1, ...), custom_call_target="tpu_custom_call" | custom-call | tf_op jit(solution)/shard_map/pallas_call | solution.py:1247
  174.6 1.0 copy.12

commit v5 on v4

--- a/solution.py
+++ b/solution.py
@@ -501,6 +501,7 @@
                 copy.wait()
 
     def remote(k, s, way, d):
+        slot = s // Y + (0, 1, Z + 1)[way]
         at = pl.ds(pl.multiple_of(s * shard, 16), part)
         if k == 0:
             ref = ff.at[:, at, 2 * hc : 3 * hc]
@@ -511,7 +512,7 @@
         else:
             ref = (g3 if k == K3 else gb).at[at]
         return pltpu.make_async_remote_copy(
-            src_ref=ref, dst_ref=ref, send_sem=zsend.at[k, way, s], recv_sem=recv.at[k, s],
+            src_ref=ref, dst_ref=ref, send_sem=zsend.at[k, slot], recv_sem=recv.at[k, s],
             device_id=d, device_id_type=MESH,
         )
 
@@ -607,8 +608,6 @@
         if q == 2:
             return pr.at[pl.ds(pl.multiple_of(first * grp, 16), count * grp)]
         at = pl.ds(pl.multiple_of(first * shard, 16), (count - 1) * shard + part)
-        if q == 3:
-            return gb.at[at]
         return gv.at[at, lead] if q == 1 else ff.at[last, at, 0:hc]
 
     def across_p(q, s):
@@ -621,7 +620,7 @@
     def remote_p(q, s, way, d):
         ref = piece(q, s * Y, Y)
         return pltpu.make_async_remote_copy(
-            src_ref=ref, dst_ref=ref, send_sem=psend.at[q, way, s], recv_sem=precv.at[q, s],
+            src_ref=ref, dst_ref=ref, send_sem=psend.at[q, s + way], recv_sem=precv.at[q, s],
             device_id=d, device_id_type=MESH,
         )
 
@@ -642,7 +641,7 @@
     def start_out(q):
         inward(lambda: left_p(q, z, go), lambda: right_p(q, z, go))
 
-    def steps_p(qs, forward):
+    def steps_p(qs, forward, first=0):
         def step(i, carry):
             @pl.when((z - 1 - i >= 0) & ((z < Z - 1) if forward else (z == Z - 1)))
             def _():
@@ -662,46 +661,26 @@
 
             return carry
 
-        lax.fori_loop(0, Z - 1, step, 0)
-
-    def inside(s):
-        return (s > 0) & (s < Z - 1)
-
-    def steps_b():
-        def step(i, carry):
-            @pl.when(z - 1 - i >= 0)
-            def _():
-                s = z - 1 - i
-
-                @pl.when(s > 0)
-                def _():
-                    remote(KB, s * Y + y, 0, dev_z(z - 1)).wait_recv()
-                    right(KB, s, go)
-                    across(KB, s, go)
-
-                @pl.when(s == 0)
-                def _():
-                    remote_p(3, s, 0, dev_z(z - 1)).wait_recv()
-                    right_p(3, s, go)
-
-            @pl.when(z + 1 + i < Z)
-            def _():
-                s = z + 1 + i
-
-                @pl.when(s < Z - 1)
-                def _():
-                    remote(KB, s * Y + y, 0, dev_z(z + 1)).wait_recv()
-                    left(KB, s, go)
-                    across(KB, s, go)
-
-                @pl.when(s == Z - 1)
-                def _():
-                    remote_p(3, s, 0, dev_z(z + 1)).wait_recv()
-                    left_p(3, s, go)
-
-            return carry
-
-        lax.fori_loop(0, Z - 1, step, 0)
+        lax.fori_loop(first, Z - 1, step, 0)
+
+    beside = jnp.where(low, 1, Z - 2)
+
+    def value_z(d):
+        ref = piece(1, beside * Y + y, 1)
+        return pltpu.make_async_remote_copy(
+            src_ref=ref, dst_ref=ref, send_sem=psend.at[1, jnp.where(low, beside + 1, beside)],
+            recv_sem=precv.at[1, beside], device_id=d, device_id_type=MESH,
+        )
+
+    def value_y(column):
+        ref = piece(1, beside * Y + column, 1)
+        return pltpu.make_async_remote_copy(
+            src_ref=ref, dst_ref=ref, send_sem=pysend.at[3], recv_sem=pyrecv.at[3],
+            device_id=dev_y, device_id_type=MESH,
+        )
+
+    def to_end():
+        return dev_z(jnp.where(low, 0, Z - 1))
 
     def pack_edges():
         packed = jnp.zeros((grp, 128), F32)
@@ -829,8 +808,8 @@
     def hidden_copy(u, kind, k):
         source = hid.at[u, 2 if kind == 2 else 0, k]
         return pltpu.make_async_remote_copy(
-            src_ref=source, dst_ref=hid.at[u, kind + 1, k], send_sem=hsem.at[0, u, kind, k],
-            recv_sem=hsem.at[1, u, kind, k], device_id=x_peer if kind == 1 else core_peer,
+            src_ref=source, dst_ref=hid.at[u, kind + 1, k], send_sem=hsem.at[0, kind, k],
+            recv_sem=hsem.at[1, kind, k], device_id=x_peer if kind == 1 else core_peer,
             device_id_type=MESH,
         )
 
@@ -841,6 +820,11 @@
         hid[u, 0, k] = (gate_v / (1.0 + jnp.exp(-gate_v)) * up_v).astype(BF16)
         hidden_copy(u, 1, k).start()
         hidden_copy(u, 0, k).start()
+
+    def hidden_sent(u):
+        for kind in range(3):
+            for k in range(nff):
+                hidden_copy(u, kind, k).wait_send()
 
     def product(u, i, k, at):
         return lax.dot_general(fd[i, k, at], hid[u, i, k], NT, preferred_element_type=F32)
@@ -909,10 +893,7 @@
         return pl.ds(pl.multiple_of(j * pair, 16), pair)
 
     def mixer_pair(r, j):
-        @pl.when(inside(j))
-        def _():
-            remote(KB, j * Y + 1 - y, 2, dev_y).wait_recv()
-
+        remote(KB, j * Y + 1 - y, 2, dev_y).wait_recv()
         at = pair_at(j)
         total = lax.dot_general(gb[at], mixed[:, 0:main], NT, preferred_element_type=F32)
         total = total + lax.dot_general(
@@ -940,7 +921,7 @@
 
     def both_squares(r, mine_sums, at):
         def arrive(s, sums):
-            tot_copy(r, at(s)).wait_recv()
+            tot_copy(r, at(s)).wait()
             return sums + squares(tot[r, column(at(s), 1 - c)].astype(F32))
 
         return mine_sums + lax.fori_loop(0, Z, arrive, jnp.zeros((8, rows), F32))
@@ -948,8 +929,8 @@
     def tot_copy(r, j):
         at = column(j, c)
         return pltpu.make_async_remote_copy(
-            src_ref=tot.at[r, at], dst_ref=tot.at[r, at], send_sem=tsem.at[0, r, j],
-            recv_sem=tsem.at[1, r, j], device_id=core_peer, device_id_type=MESH,
+            src_ref=tot.at[r, at], dst_ref=tot.at[r, at], send_sem=tsem.at[0, j],
+            recv_sem=tsem.at[1, j], device_id=core_peer, device_id_type=MESH,
         )
 
     def toward():
@@ -961,16 +942,8 @@
         return jnp.where(s <= 2 * near, close, jnp.where(low, s, Z - 1 - s))
 
     def pass_on(j):
-        source = toward()
-
-        @pl.when(inside(j))
-        def _():
-            remote(KB, j * Y + y, 0, source).wait_recv()
-            across(KB, j, go)
-
-        @pl.when(~inside(j))
-        def _():
-            remote_p(3, j, 0, source).wait_recv()
+        remote(KB, j * Y + y, 0, toward()).wait_recv()
+        across(KB, j, go)
 
     def end_steps(first, stop):
         source = toward()
@@ -1067,40 +1040,40 @@
                 across(k, s, done)
                 return carry
 
-            lax.fori_loop(*((0, Z) if k < KB else (1, Z - 1)), drain, 0)
-        for q in range(4):
+            lax.fori_loop(0, Z, drain, 0)
+        for q in range(3):
             def drain_p(s, carry):
-                @pl.when((s <= z) & ((q < 3) | ~inside(s)))
+                alone = (s == z) & ~at_end if q == 1 else s < 0
+
+                @pl.when((s <= z) & ~(alone & ~low))
                 def _():
                     right_p(q, s, done)
 
-                @pl.when((s >= z) & ((q < 3) | ~inside(s)))
+                @pl.when((s >= z) & ~(alone & low))
                 def _():
                     left_p(q, s, done)
 
                 return carry
 
             lax.fori_loop(0, Z, drain_p, 0)
-        for q in range(3):
             across_p(q, f).wait_send()
 
         @pl.when(at_end)
         def _():
-            across_p(3, f).wait_send()
+            value_y(y).wait_send()
+
+        @pl.when(~at_end)
+        def _():
+            value_z(to_end()).wait_send()
 
         def drain_r(s, carry):
             core_copy(1, s).wait_send()
             x_copy(1, s).wait_send()
-            for r in range(2):
-                tot_copy(r, s).wait_send()
             for v in range(Y):
                 spread(s, v, done)
             return carry
 
         lax.fori_loop(0, Z, drain_r, 0)
-        for kind in range(3):
-            for k in range(nff):
-                hidden_copy(0, kind, k).wait_send()
 
     def spread_across(s, carry):
         j = order(s)
@@ -1124,8 +1097,7 @@
 
     @pl.when(at_end)
     def _():
-        across_p(3, f).start()
-        for k in range(2, K3 + 1):
+        for k in range(2, KB + 1):
             own_in(k)
 
     own_out(2)
@@ -1147,7 +1119,7 @@
 
     @pl.when(at_end)
     def _():
-        for q in range(1, 4):
+        for q in range(1, 3):
             start_in(q)
 
     zsteps(1)
@@ -1178,12 +1150,12 @@
     @pl.when(~at_end)
     def _():
         zsteps(K3)
-        start_out(1)
+        value_z(to_end()).start()
         start_out(2)
         steps_p((1, 2), True)
         own_out(KB)
         own_y(KB)
-        steps_b()
+        zsteps(KB)
 
     wait_across(2)
     hidden(0, 1)
@@ -1201,9 +1173,22 @@
     sums = finish_ffn(0, 0, lambda: end_steps(2, Z - 1), None)
     norm_to(res.at[0], update(0, sums, xt, 1, 0.5), 2)
     end_steps(Z - 1, Z)
+
+    @pl.when(at_end)
+    def _():
+        value_z(toward()).wait_recv()
+        value_y(y).start()
+        own_y(KB)
+
+    hidden_sent(0)
     wait_across(K3)
     unpack_edges()
-    steps_p((1,), False)
+    steps_p((1,), False, 1)
+
+    @pl.when(at_end)
+    def _():
+        value_y(1 - y).wait_recv()
+
     mixer()
     sums = reduce(1, mixer_pair)
     norm_to(res.at[1], update(1, sums, res.at[0], 3, 1.0), 4)
@@ -1218,14 +1203,7 @@
         at = pl.ds(s * shard, part)
         v = res[1, at].astype(F32) + tot[2, at].astype(F32) * scale * gain_block(5, at)
         out_ref[s * part : (s + 1) * part] = v.astype(BF16)
-    def drain_last(j, carry):
-        tot_copy(2, j).wait_send()
-        return carry
-
-    lax.fori_loop(0, Z, drain_last, 0)
-    for kind in range(3):
-        for k in range(nff):
-            hidden_copy(1, kind, k).wait_send()
+    hidden_sent(1)
 
 
 def stream_form(mesh, Z):
@@ -1275,17 +1253,17 @@
                 vmem((4, nff, Z * shard, hc), BF16),
                 vmem((Z * shard, rows), F32),
                 dma((3 * nff + 10 + n_fs,)),
-                dma((nff + 3, 3, n_fs)),
+                dma((nff + 3, 2 * Z + 1)),
                 dma((nff + 3, n_fs)),
-                dma((4, 2, Z)),
+                dma((4, Z + 1)),
                 dma((4, Z)),
                 dma((4,)),
                 dma((4,)),
                 dma((2, Z)),
                 dma((2, Z)),
+                dma((2, Z)),
                 dma((2, 3, Z)),
-                dma((2, 3, Z)),
-                dma((2, 2, 3, nff)),
+                dma((2, 3, nff)),
             ],
             compiler_params=pltpu.CompilerParams(
                 collective_id=0, has_side_effects=True, vmem_limit_bytes=60 * 1024 * 1024
@@ -1382,7 +1360,7 @@
         rem = channels % 128
         fits = Y == 2 and X == 2 and part % 8 == 0 and 0 < rem <= 8 and rows % 128 == 0
         fits = fits and (n_fs * (-(-part // 16) * 16)) % 128 == 0 and channels > 128
-        fits = fits and args[2].shape[1] % 384 == 0 and Z > 2
+        fits = fits and args[2].shape[1] % 384 == 0 and Z == 4
         return (stream_form(mesh, Z) if fits else chain_form)(*args)
 
     return jax.shard_map(

time: 176 us -> 173 us (0.983)
  Pallas kernels: 175 us -> 172 us
    pallas_call x1, Pallas kernels: 175 us -> 172 us  [local(): pl.pallas_call(functools.partial(stream_kernel, (Z, shard, part, width, h...]
where the time goes in v5:
time: 173 us
  Pallas kernels  172 us (99%)
    pallas_call x1, Pallas kernels, local(): pl.pallas_call(functools.partial(stream_kernel, (Z, shard, part, width, h...  172 us

profile of v5, /device:TPU:0, one launch (start us, length us, event | category | flops | bytes accessed | tf_op | source)
XLA Modules:
  0.0 172.9 jit_solution(3944918893555114888)
XLA Ops:
  0.0 171.9 %shard_map.100 = bf16[2112,256]{1,0:T(8,128)(2,1)S(1)} custom-call(bf16[264,768]{1,0:T(8,128)(2,1)} %refs_0_.1, bf16[264,768]{1,0:T(8,128)(2,1)} %refs_1_.1, bf16[264,768]{1,0:T(8,128)(2,1)} %refs_2_.1, bf16[264,264]{1,0:T(8,128)(2,1)} %refs_3_.1, bf16[264,264]{1,0:T(8,128)(2,1)} %refs_4_.1, bf16[264,264]{1,0:T(8,128)(2,1)} %refs_5_.1, ...), custom_call_target="tpu_custom_call" | custom-call | tf_op jit(solution)/shard_map/pallas_call | solution.py:1225
  172.0 1.0 copy.12

commit v6 on v5

--- a/solution.py
+++ b/solution.py
@@ -468,9 +468,6 @@
                 for k in range(nff):
                     clear(fd, (i, k, pad))
 
-    for owner, copy in local:
-        if owner < 2:
-            copy.start()
     clear_pairs()
     barrier = pltpu.get_barrier_semaphore()
 
@@ -488,9 +485,8 @@
     def _():
         greet(dev_z(z + 1))
 
-    for owner, copy in local:
-        if owner >= 2:
-            copy.start()
+    for _, copy in local:
+        copy.start()
     clear_rest()
     peers = 4 + (z > 0).astype(jnp.int32) + (z < Z - 1).astype(jnp.int32)
     pl.semaphore_wait(barrier, peers)

time: 173 us -> 173 us (level)
  no operation moved by 1% of the time
where the time goes in v6:
time: 173 us
  Pallas kernels  172 us (99%)
    pallas_call x1, Pallas kernels, local(): pl.pallas_call(functools.partial(stream_kernel, (Z, shard, part, width, h...  172 us

profile of v6, /device:TPU:0, one launch (start us, length us, event | category | flops | bytes accessed | tf_op | source)
XLA Modules:
  0.0 173.0 jit_solution(3117574463698182854)
XLA Ops:
  0.0 172.0 %shard_map.100 = bf16[2112,256]{1,0:T(8,128)(2,1)S(1)} custom-call(bf16[264,768]{1,0:T(8,128)(2,1)} %refs_0_.1, bf16[264,768]{1,0:T(8,128)(2,1)} %refs_1_.1, bf16[264,768]{1,0:T(8,128)(2,1)} %refs_2_.1, bf16[264,264]{1,0:T(8,128)(2,1)} %refs_3_.1, bf16[264,264]{1,0:T(8,128)(2,1)} %refs_4_.1, bf16[264,264]{1,0:T(8,128)(2,1)} %refs_5_.1, ...), custom_call_target="tpu_custom_call" | custom-call | tf_op jit(solution)/shard_map/pallas_call | solution.py:1221
  172.0 1.0 copy.12
